TPU v7x, 32 devices: a whole 2x2x4 slice. The times are simulated.
32 devices in a mesh: rep: 1, fs: 16 (over z, y, x), tp: 2 (over core).
Axes of the slice: x: 2, y: 2, z: 4, core: 2. Of those that a mesh axis runs over, the one named last changes fastest.
Arguments:
- sequence: bfloat16 [16, 768, 2048], P(('rep', 'fs'), None, 'tp'), may hold values from -6 to 6
- mix_gain: float32 [2048], replicated, may hold values from 0.1 to 1.9
- ffn_gain: float32 [2048], replicated, may hold values from 0.1 to 1.9
- proj_outer: float32 [2048, 2048], P(None, ('tp', 'fs')), may hold values from -0.125 to 0.125
- proj_inner: float32 [2048, 2048], P(None, ('tp', 'fs')), may hold values from -0.125 to 0.125
- proj_value: float32 [2048, 2048], P(None, ('tp', 'fs')), may hold values from -0.125 to 0.125
- proj_scales: float32 [3, 2048], P(None, 'tp'), may hold values from 0.5 to 2
- taps: float32 [3, 2048], P(None, 'tp'), may hold values from -3 to 3
- mix_out: float32 [2048, 2048], P('tp', 'fs'), may hold values from -0.125 to 0.125
- mix_out_scale: float32 [2048], P('fs'), may hold values from 0.5 to 2
- ffn_gate: float32 [2048, 2816], P(None, ('tp', 'fs')), may hold values from -0.125 to 0.125
- ffn_up: float32 [2048, 2816], P(None, ('tp', 'fs')), may hold values from -0.125 to 0.125
- ffn_scales: float32 [2, 2816], P(None, 'tp'), may hold values from 0.5 to 2
- ffn_down: float32 [2816, 2048], P('tp', 'fs'), may hold values from -0.109375 to 0.109375
- down_scale: float32 [2048], P('fs'), may hold values from 0.5 to 2
Outputs:
- layer_out: bfloat16 [16, 768, 2048], P(('rep', 'fs'), None, 'tp')
All inputs are finite; a program needn't handle non-finite values.
Results may differ from a plain program's by a relative error of at most 0.013.
Values may be sent and summed in bfloat16 or wider, within the bound.
A program may use at most 128 MiB of HBM per device.

v0:
```python
import functools
import math

import jax
import jax.numpy as jnp
from jax import lax
from jax.experimental import pallas as pl
from jax.experimental.pallas import tpu as pltpu
from jax.sharding import PartitionSpec as P

eps = 1e-06
MESH = pl.DeviceIdType.MESH
BF16 = jnp.bfloat16
F32 = jnp.float32
Z, Y, X = 0, 1, 2
ROWS = 256


def grid_of(n):
    side = 2 ** round(math.log2(n) / 3) if n > 1 else 1
    if n % (side * side):
        side = 1
    return (n // (side * side), side, side)


def routes(dims, order):
    found = []
    frontier = [((0, 0, 0), None, 0, 0)]
    while frontier:
        offset, last, way, depth = frontier.pop(0)
        for place, axis in enumerate(order):
            down = 0 if dims[axis] == 2 else dims[axis] - 1
            for step, limit in ((1, dims[axis] - 1), (-1, down)):
                if last is not None and place < last:
                    continue
                if last == place and step != way:
                    continue
                if abs(offset[axis] + step) > limit:
                    continue
                child = list(offset)
                child[axis] += step
                child = tuple(child)
                found.append((child, offset, axis, step, depth + 1))
                frontier.append((child, place, step, depth + 1))
    return found


def product(rows, columns):
    return lax.dot_general(
        rows, columns, (((1,), (1,)), ((), ())), preferred_element_type=F32
    )


def layer_kernel(
    dims,
    seq,
    p_in,
    m_in,
    g_in,
    d_in,
    chan,
    gains,
    hid,
    out,
    pbuf,
    mbuf,
    gbuf,
    dbuf,
    both,
    nbuf,
    gated,
    ext,
    hbuf,
    dsend,
    drecv,
    xsend,
    xrecv,
    frecv,
    w_send,
    w_recv,
    own_sem,
    s_send,
    s_recv,
    x_send,
    x_recv,
    c_send,
    c_recv,
):
    me = lax.axis_index("fs")
    core = lax.axis_index("tp")
    peer = {"tp": 1 - core}
    xp = lax.rem(me, 2)
    partner = {"fs": me + 1 - 2 * xp}
    group = me // 2
    place = (
        group // (dims[1] * dims[2]),
        lax.rem(group // dims[2], dims[1]),
        lax.rem(group, dims[2]),
    )
    members = dims[0] * dims[1] * dims[2]
    length, width = seq.shape
    chunks = length // ROWS
    kch = p_in.shape[2]
    fch = g_in.shape[1]
    cols = m_in.shape[1] - 16
    pair = 2 * cols
    wide = kch * members
    hidden = fch * members
    origin = (0, 0, 0)

    def index(offset):
        at = [lax.rem(place[k] + offset[k] + dims[k], dims[k]) for k in range(3)]
        return (at[0] * dims[1] + at[1]) * dims[2] + at[2]

    def slot_of(offset):
        at = [offset[k] % dims[k] for k in range(3)]
        return (at[0] * dims[1] + at[1]) * dims[2] + at[2]

    def shifted(axis, step):
        return 2 * index(tuple(step if k == axis else 0 for k in range(3))) + xp

    def within(pairs):
        holds = None
        for axis, step in sorted(set(pairs)):
            if dims[axis] == 2 or step == 0:
                continue
            at = place[axis] + step
            one = (at >= 0) if step < 0 else (at < dims[axis])
            holds = one if holds is None else jnp.logical_and(holds, one)
        return holds

    def guarded(holds, act):
        if holds is None:
            act()
        else:
            pl.when(holds)(act)

    def of(step, size):
        return pl.ds(pl.multiple_of(step * size, size), size)

    cut = pair * 2 // 3 // 16 * 16
    views = [
        lambda i: pbuf.at[0, :, of(i, kch)],
        lambda i: pbuf.at[1, :, of(i, kch)],
        lambda i: mbuf.at[i],
        lambda i: gbuf.at[0, of(i, fch)],
        lambda i: gbuf.at[1, of(i, fch)],
        lambda i: dbuf.at[i, pl.ds(0, cut)],
        lambda i: dbuf.at[i, pl.ds(cut, pair - cut)],
    ]
    inputs = {0: p_in.at[0], 1: p_in.at[1], 3: g_in.at[0], 4: g_in.at[1]}
    orders = [(Z, X, Y), (Z, X, Y), (Y, X, Z), (Z, X, Y), (Z, X, Y), (Z, X, Y), (Y, X, Z)]
    plans = [routes(dims, order) for order in orders]
    base = [sum(len(p) for p in plans[:k]) for k in range(len(plans))]
    arrived = [set() for _ in plans]
    sent = []

    def copy_of(part, number):
        child, parent, axis, step, _ = plans[part][number]
        home = views[part](index(parent))
        return pltpu.make_async_remote_copy(
            src_ref=inputs[part] if parent == origin and part in inputs else home,
            dst_ref=home,
            send_sem=w_send.at[base[part] + number],
            recv_sem=w_recv.at[part, slot_of(child)],
            device_id={"fs": shifted(axis, -step)},
            device_id_type=MESH,
        )

    def launch(part, parent):
        for number, item in enumerate(plans[part]):
            if item[1] == parent:
                holds = within(list(enumerate(parent)) + [(item[2], -item[3])])
                guarded(holds, copy_of(part, number).start)
                sent.append((part, number, holds))

    def arrive(part, child):
        if child in arrived[part]:
            return
        arrived[part].add(child)
        block = views[part](index(child))
        ahead = [k for k in range(3) if dims[k] > 1][0]
        there = pltpu.make_async_remote_copy(
            src_ref=block,
            dst_ref=block,
            send_sem=w_send.at[0],
            recv_sem=w_recv.at[part, slot_of(child)],
            device_id={"fs": shifted(ahead, 1)},
            device_id_type=MESH,
        )
        guarded(within(list(enumerate(child))), there.wait_recv)

    def parents(part, depth):
        found = []
        for child, parent, axis, step, level in plans[part]:
            if level == depth + 1 and parent not in found:
                found.append(parent)
        return found

    def relay(part, depth):
        for parent in parents(part, depth):
            arrive(part, parent)
            launch(part, parent)

    def finish(part):
        for item in plans[part]:
            arrive(part, item[0])

    deepest = [max(item[4] for item in p) for p in plans]

    near = [(axis, 1) for axis in range(3) if dims[axis] > 1]
    near += [(axis, -1) for axis in range(3) if dims[axis] > 2]
    barrier = pltpu.get_barrier_semaphore()
    for axis, step in near:
        pl.semaphore_signal(
            barrier, inc=1, device_id={"fs": shifted(axis, step)}, device_id_type=MESH
        )
    pl.semaphore_signal(barrier, inc=1, device_id=partner, device_id_type=MESH)
    pl.semaphore_signal(barrier, inc=1, device_id=peer, device_id_type=MESH)
    pl.semaphore_wait(barrier, len(near) + 2)

    def to(where, src, dst, send, recv):
        return pltpu.make_async_remote_copy(
            src_ref=src,
            dst_ref=dst,
            send_sem=send,
            recv_sem=recv,
            device_id=where,
            device_id_type=MESH,
        )

    mine = of(core, width)
    theirs = of(1 - core, width)

    def rows(r):
        return of(r, ROWS)

    seq_local = pltpu.make_async_copy(seq, both.at[0, :, mine], own_sem.at[0])
    seq_peer = to(peer, seq, both.at[0, :, mine], s_send.at[0], s_recv.at[0])
    seq_partner = [
        to(
            partner,
            seq.at[pl.ds(r * ROWS, ROWS)],
            both.at[1, pl.ds(r * ROWS, ROWS), mine],
            s_send.at[1 + r],
            s_recv.at[1 + r],
        )
        for r in range(chunks)
    ]
    seq_pass = [
        to(
            peer,
            both.at[1, pl.ds(r * ROWS, ROWS), mine],
            both.at[1, pl.ds(r * ROWS, ROWS), mine],
            s_send.at[1 + chunks + r],
            s_recv.at[1 + chunks + r],
        )
        for r in range(chunks)
    ]
    cross = []
    locals_ = [seq_local]
    side = of(xp, cols)
    tail = pl.ds(pl.multiple_of(pair + xp * 16, 16), 16)
    for k, (src, dst) in enumerate(
        (
            (lambda t: m_in.at[t, pl.ds(0, cols)], mbuf.at[group, side]),
            (lambda t: m_in.at[t, pl.ds(cols, 16)], mbuf.at[group, tail]),
            (lambda t: d_in.at[t], dbuf.at[group, side]),
        )
    ):
        at = 1 + 2 * chunks + k
        cross.append(to(partner, src(1 - xp), dst, s_send.at[at], s_recv.at[at]))
        locals_.append(pltpu.make_async_copy(src(xp), dst, own_sem.at[1 + k]))
    for k, part in enumerate(sorted(inputs)):
        locals_.append(
            pltpu.make_async_copy(inputs[part], views[part](group), own_sem.at[4 + k])
        )

    launch(0, origin)
    for copy in seq_partner:
        copy.start()
    seq_peer.start()
    for copy in locals_:
        copy.start()
    for copy in cross:
        copy.start()
    launch(1, origin)

    def norm(s, first, count, gain):
        tall = 16

        def step(i, _):
            at = pl.ds(pl.multiple_of(first + i * tall, tall), tall)
            values = both[s, at, :].astype(F32)
            mean = jnp.mean(values * values, axis=-1, keepdims=True)
            scaled = values * lax.rsqrt(mean + eps)
            nbuf[s, at, :] = (scaled * gains[pl.ds(gain, 1), :]).astype(BF16)
            return 0

        lax.fori_loop(0, count // tall, step, 0)

    def project(k, s):
        ext[0:8, :] = jnp.zeros((8, wide), F32)

        def step(r, _):
            block = nbuf[s, rows(r), :]
            inner = product(block, pbuf[k, 1]) * chan[k, 1:2, :]
            value = product(block, pbuf[k, 2]) * chan[k, 2:3, :]
            carried = inner * value
            ext[8 : 8 + ROWS, :] = carried
            conv = chan[k, 3:4, :] * ext[6 : 6 + ROWS, :]
            conv = conv + chan[k, 4:5, :] * ext[7 : 7 + ROWS, :]
            conv = conv + chan[k, 5:6, :] * carried
            ext[0:8, :] = ext[ROWS : ROWS + 8, :]
            outer = product(block, pbuf[k, 0]) * chan[k, 0:1, :]
            gated[s, rows(r), pl.ds(k * wide, wide)] = (outer * conv).astype(BF16)
            return 0

        lax.fori_loop(0, chunks, step, 0)

    def exchange(kind, s, r):
        at = kind * 2 * chunks + s * chunks + r
        home = drecv.at[s, rows(r)]
        return to(peer, dsend.at[s, rows(r)], home, c_send.at[at], c_recv.at[at])

    def spread(s, r):
        at = 4 * chunks + s * chunks + r
        home = both.at[s, rows(r), mine]
        return to(peer, home, home, c_send.at[at], c_recv.at[at])

    def crossing(s, r):
        return to(
            partner,
            xsend.at[s, rows(r)],
            xrecv.at[1 - s, rows(r)],
            x_send.at[s * chunks + r],
            x_recv.at[(1 - s) * chunks + r],
        )

    def crossed(s, r):
        return to(
            partner,
            xsend.at[s, rows(r)],
            xrecv.at[s, rows(r)],
            x_send.at[s * chunks + r],
            x_recv.at[s * chunks + r],
        )

    def last(r):
        at = 2 * chunks + r
        return to(
            partner, xsend.at[1, rows(r)], frecv.at[rows(r)], x_send.at[at], x_recv.at[at]
        )

    half = members // 2

    def scale_of(g, which):
        scale = jnp.zeros((1, pair), F32)
        for side_ in range(2):
            tile = mbuf[g, pl.ds(pair + 16 * side_, 16), pl.ds(0, pair)].astype(F32)
            for k in range(3):
                scale = scale + tile[3 * which + k : 3 * which + k + 1]
        return scale

    def partial(rows_value, buf, which, s, r):
        def away(i, _):
            g = (1 - core) * half + i
            term = product(rows_value(), buf[g, pl.ds(0, pair), :]) * scale_of(g, which)
            dsend[s, rows(r), of(i, pair)] = term.astype(BF16)
            return 0

        def keep(i, _):
            g = core * half + i
            term = product(rows_value(), buf[g, pl.ds(0, pair), :]) * scale_of(g, which)
            xsend[s, rows(r), of(i, pair)] = term.astype(BF16)
            return 0

        lax.fori_loop(0, half, away, 0)
        exchange(which, s, r).start()
        lax.fori_loop(0, half, keep, 0)

    def each(act):
        def step(r, _):
            act(r)
            return 0

        lax.fori_loop(0, chunks, step, 0)

    def mix_terms(s):
        each(lambda r: partial(lambda: gated[s, rows(r), :], mbuf, 0, s, r))

    def add_peer(which, s, r):
        copy = exchange(which, s, r)
        copy.wait_recv()
        total = xsend[s, rows(r), :].astype(F32) + drecv[s, rows(r), :].astype(F32)
        xsend[s, rows(r), :] = total.astype(BF16)
        copy.wait_send()

    def mix_cross(s):
        def act(r):
            add_peer(0, s, r)
            crossing(s, r).start()

        each(act)

    def mix_after(s):
        def act(r):
            crossed(s, r).wait_recv()
            mix = xsend[s, rows(r), :].astype(F32) + xrecv[s, rows(r), :].astype(F32)
            after = both[s, rows(r), mine].astype(F32) + mix
            both[s, rows(r), mine] = after.astype(BF16)
            spread(s, r).start()
            crossing(s, r).wait_send()

        each(act)

    def feed(s):
        def act(r):
            spread(s, r).wait_recv()
            norm(s, r * ROWS, ROWS, 1)
            block = nbuf.at[s, rows(r)]

            def unit(i, _):
                at = of(i, wide)
                gate = product(block[...], gbuf[0, at, :]) * hid[0:1, at]
                up = product(block[...], gbuf[1, at, :]) * hid[1:2, at]
                hbuf[:, at] = (gate / (1.0 + jnp.exp(-gate)) * up).astype(BF16)
                return 0

            lax.fori_loop(0, hidden // wide, unit, 0)
            partial(lambda: hbuf[...], dbuf, 1, s, r)

        each(act)

    def feed_cross():
        def act(r):
            add_peer(1, 1, r)
            last(r).start()

        each(act)

    def close():
        def act(r):
            copy = exchange(1, 0, r)
            copy.wait_recv()
            last(r).wait_recv()
            ffn = xsend[0, rows(r), :].astype(F32) + drecv[0, rows(r), :].astype(F32)
            ffn = ffn + frecv[rows(r), :].astype(F32)
            after = both[0, rows(r), mine].astype(F32)
            out[rows(r), :] = (after + ffn).astype(BF16)
            copy.wait_send()

        each(act)

    seq_local.wait()
    seq_peer.wait_recv()
    norm(0, 0, length, 0)
    for depth in range(1, deepest[0]):
        relay(0, depth)
        if depth <= chunks:
            seq_partner[depth - 1].wait_recv()
            seq_pass[depth - 1].start()
    for r in range(deepest[0] - 1, chunks):
        seq_partner[r].wait_recv()
        seq_pass[r].start()
    for copy in locals_[1:4]:
        copy.wait()
    for copy in cross:
        copy.wait_recv()
    launch(2, origin)
    relay(1, 1)
    finish(0)
    for copy in locals_[4:]:
        copy.wait()
    project(0, 0)
    relay(1, 2)
    for copy in seq_pass:
        copy.wait()
    norm(1, 0, length, 0)
    launch(3, origin)
    for depth in range(3, deepest[1]):
        relay(1, depth)
    relay(2, 1)
    project(0, 1)
    for depth in range(2, deepest[2]):
        relay(2, depth)
    finish(1)
    project(1, 1)
    relay(3, 1)
    launch(4, origin)
    project(1, 0)
    relay(3, 2)
    finish(2)
    mix_terms(1)
    mix_cross(1)
    for depth in range(3, deepest[3]):
        relay(3, depth)
    relay(4, 1)
    mix_terms(0)
    mix_cross(0)
    launch(6, origin)
    launch(5, origin)
    relay(4, 2)
    for depth in range(1, deepest[6]):
        relay(6, depth)
    for depth in range(3, deepest[4]):
        relay(4, depth)
    relay(5, 1)
    mix_after(1)
    for depth in range(2, deepest[5]):
        relay(5, depth)
    finish(3)
    finish(4)
    finish(5)
    finish(6)
    feed(1)
    mix_after(0)
    feed_cross()
    feed(0)
    close()
    for part, number, holds in sent:
        guarded(holds, copy_of(part, number).wait_send)
    seq_peer.wait_send()
    for copy in seq_partner + cross:
        copy.wait_send()
    for s in range(2):
        each(lambda r: spread(s, r).wait_send())
    each(lambda r: last(r).wait_send())


def prepare(
    n,
    proj_outer,
    proj_inner,
    proj_value,
    proj_scales,
    taps,
    mix_out,
    mix_out_scale,
    ffn_gate,
    ffn_up,
    ffn_scales,
    ffn_down,
    down_scale,
):
    half = n // 2
    xp = lax.rem(lax.axis_index("fs"), 2)
    each = proj_outer.shape[1]
    kch = each // 2
    p_in = jnp.stack(
        [w.astype(BF16).T.reshape(2, kch, -1) for w in (proj_outer, proj_inner, proj_value)],
        axis=1,
    )
    units = ffn_gate.shape[1]
    fill = -units % 16
    g_in = jnp.stack(
        [jnp.pad(w.astype(BF16).T, ((0, fill), (0, 0))) for w in (ffn_gate, ffn_up)]
    )
    cols = mix_out.shape[1]
    mixed = mix_out.astype(BF16).T.reshape(cols, half, 2, 2, kch)
    mixed = mixed.transpose(2, 0, 3, 1, 4).reshape(2, cols, half * each)
    thin = []
    for scale in (mix_out_scale, down_scale):
        high = lax.reduce_precision(scale, 8, 7)
        middle = lax.reduce_precision(scale - high, 8, 7)
        thin += [high, middle, scale - high - middle]
    thin = jnp.stack(thin)
    ours = (lax.iota(jnp.int32, 2 * cols) // cols == xp)[None]
    thin = jnp.where(ours, jnp.concatenate([thin, thin], 1), 0.0).astype(BF16)
    thin = jnp.pad(thin, ((0, 10), (0, half * each - 2 * cols)))
    m_in = jnp.concatenate([mixed, jnp.broadcast_to(thin, (2,) + thin.shape)], axis=1)
    down = ffn_down.astype(BF16).T.reshape(cols, half, 2, units)
    d_in = jnp.pad(down, ((0, 0), (0, 0), (0, 0), (0, fill))).transpose(2, 0, 1, 3)
    d_in = d_in.reshape(2, cols, -1)
    chan = jnp.concatenate([proj_scales, taps]).reshape(6, half, 2, 2, kch)
    chan = lax.dynamic_index_in_dim(chan, xp, 2, keepdims=False)
    chan = chan.transpose(2, 0, 1, 3).reshape(2, 6, half * kch)
    chan = jnp.pad(chan, ((0, 0), (0, 2), (0, 0)))
    hid = ffn_scales.reshape(2, half, 2, units)
    hid = lax.dynamic_index_in_dim(hid, xp, 2, keepdims=False)
    hid = jnp.pad(hid, ((0, 6), (0, 0), (0, fill))).reshape(8, -1)
    return p_in, m_in, g_in, d_in, chan, hid


def body(n, sequence, mix_gain, ffn_gain, *rest):
    seq = sequence[0]
    length, width = seq.shape
    depth = 2 * width
    p_in, m_in, g_in, d_in, chan, hid = prepare(n, *rest)
    gains = jnp.pad(jnp.stack([mix_gain, ffn_gain]), ((0, 6), (0, 0)))
    full = grid_of(n)
    dims = (full[0], full[1], full[2] // 2)
    members = n // 2
    kch, fch = p_in.shape[2], g_in.shape[1]
    cols = m_in.shape[1] - 16
    chunks = length // ROWS
    items = 7 * len(routes(dims, (Z, X, Y))) + 2 * members * 7
    operands = (seq, p_in, m_in, g_in, d_in, chan, gains, hid)
    result = pl.pallas_call(
        functools.partial(layer_kernel, dims),
        out_shape=jax.ShapeDtypeStruct(seq.shape, BF16),
        in_specs=[pl.BlockSpec(memory_space=pltpu.VMEM)] * len(operands),
        out_specs=pl.BlockSpec(memory_space=pltpu.VMEM),
        scratch_shapes=[
            pltpu.VMEM((2, 3, members * kch, depth), BF16),
            pltpu.VMEM((members, 2 * cols + 32, m_in.shape[2]), BF16),
            pltpu.VMEM((2, members * fch, depth), BF16),
            pltpu.VMEM((members, 2 * cols, d_in.shape[2]), BF16),
            pltpu.VMEM((2, length, depth), BF16),
            pltpu.VMEM((2, length, depth), BF16),
            pltpu.VMEM((2, length, m_in.shape[2]), BF16),
            pltpu.VMEM((8 + ROWS, members * kch), F32),
            pltpu.VMEM((ROWS, members * fch), BF16),
            pltpu.VMEM((2, length, width), BF16),
            pltpu.VMEM((2, length, width), BF16),
            pltpu.VMEM((2, length, width), BF16),
            pltpu.VMEM((2, length, width), BF16),
            pltpu.VMEM((length, width), BF16),
            pltpu.SemaphoreType.DMA((items,)),
            pltpu.SemaphoreType.DMA((7, members)),
            pltpu.SemaphoreType.DMA((8,)),
            pltpu.SemaphoreType.DMA((4 + 2 * chunks,)),
            pltpu.SemaphoreType.DMA((4 + 2 * chunks,)),
            pltpu.SemaphoreType.DMA((3 * chunks,)),
            pltpu.SemaphoreType.DMA((3 * chunks,)),
            pltpu.SemaphoreType.DMA((6 * chunks,)),
            pltpu.SemaphoreType.DMA((6 * chunks,)),
        ],
        compiler_params=pltpu.CompilerParams(
            collective_id=0, has_side_effects=True, vmem_limit_bytes=67043328
        ),
        name="layer",
    )(*operands)
    return result[None]


def solution(mesh):
    in_specs = (
        P(("rep", "fs"), None, "tp"),
        P(),
        P(),
        P(None, ("tp", "fs")),
        P(None, ("tp", "fs")),
        P(None, ("tp", "fs")),
        P(None, "tp"),
        P(None, "tp"),
        P("tp", "fs"),
        P("fs"),
        P(None, ("tp", "fs")),
        P(None, ("tp", "fs")),
        P(None, "tp"),
        P("tp", "fs"),
        P("fs"),
    )
    out_specs = P(("rep", "fs"), None, "tp")
    return jax.shard_map(
        functools.partial(body, mesh.shape["fs"]),
        mesh=mesh,
        in_specs=in_specs,
        out_specs=out_specs,
        check_vma=False,
    )
```

profile of v0, /device:TPU:0, one launch (start us, length us, event | category | flops | bytes accessed | tf_op | source)
XLA Modules:
  0.0 275.8 jit_solution(1137797084611862735)
XLA Ops:
  0.0 0.8 fusion.2
  0.8 0.8 reshape.44
  1.7 0.7 reshape.45.hid
  2.4 0.7 pad_maximum_fusion.3
  3.1 0.1 reshape.42
  3.3 0.1 reshape.43
  3.4 0.6 pad.31.chan
  4.0 1.4 select_maximum_fusion.gains
  5.3 1.1 convert_element_type.37
  6.4 0.0 copy-done.3
  6.4 0.0 copy-start.5
  6.5 0.0 copy-done.4
  6.5 1.0 pad_maximum_fusion.p_in
  7.6 0.1 copy.24
  7.7 0.8 pad_maximum_fusion.2.m_in
  8.5 0.1 copy-done
  8.7 0.3 copy-done.1
  9.0 0.0 copy-start.2
  9.0 0.1 pad_bitcast_fusion.1
  9.1 1.0 pad_maximum_fusion.1.g_in
  10.0 0.1 copy-done.2
  10.3 0.9 copy.28.d_in
  11.2 261.9 %layer.1 = bf16[768,1024]{1,0:T(8,128)(2,1)} custom-call(bf16[768,1024]{1,0:T(8,128)(2,1)} %bitcast.57, bf16[2,3,32,2048]{3,2,1,0:T(8,128)(2,1)} %pad_maximum_fusion.p_in, bf16[2,144,512]{2,1,0:T(8,128)(2,1)} %pad_maximum_fusion.2.m_in, bf16[2,96,2048]{2,1,0:T(8,128)(2,1)} %pad_maximum_fusion.1.g_in, bf16[2,128,768]{2,1,0:T(8,128)(2,1)} %copy.28.d_in, ...), custom_call_target="tpu_custom_call" | custom-call | tf_op jit(solution)/shard_map/layer/pallas_call | solution.py:599
  273.1 2.7 copy.32
  (24 shorter events, 0.4 us)
Async XLA Ops:
  0.0 6.5 %copy-start.4 = (f32[2048,64]{0,1:T(8,128)S(1)}, f32[2048,64]{0,1:T(8,128)}, u32[]{:S(2)}) copy-start(f32[2048,64]{0,1:T(8,128)} %param.20) | copy-start | bytes 1572868
  0.0 6.4 %copy-start.3 = (f32[2048,64]{0,1:T(8,128)S(1)}, f32[2048,64]{0,1:T(8,128)}, u32[]{:S(2)}) copy-start(f32[2048,64]{0,1:T(8,128)} %param.19) | copy-start | bytes 1572868
  6.4 1.1 copy-start.5
  7.5 1.1 copy-start
  7.5 1.4 copy-start.1
  9.0 1.2 copy-start.2
where the time goes:
time: 276 us
  Pallas kernels  262 us (95%)
  local copies, waits for them, and re-layouts  6.85 us (2%)
  other arithmetic  6.84 us (2%)
    pallas_call x1, Pallas kernels, body(): pl.pallas_call(functools.partial(layer_kernel, dims), out_shape=jax.Shape...  262 us

commit v1 on v0

v1 whole, which is shorter than its diff:
```python
import functools
import math

import jax
import jax.numpy as jnp
from jax import lax
from jax.experimental import pallas as pl
from jax.experimental.pallas import tpu as pltpu
from jax.sharding import PartitionSpec as P

eps = 1e-06
MESH = pl.DeviceIdType.MESH
BF16 = jnp.bfloat16
F32 = jnp.float32
Z, Y, X = 0, 1, 2
ROWS = 256


def grid_of(n):
    side = 2 ** round(math.log2(n) / 3) if n > 1 else 1
    if n % (side * side):
        side = 1
    return (n // (side * side), side, side)


def routes(dims, order):
    found = []
    frontier = [((0, 0, 0), None, 0, 0)]
    while frontier:
        offset, last, way, depth = frontier.pop(0)
        for place, axis in enumerate(order):
            down = 0 if dims[axis] == 2 else dims[axis] - 1
            for step, limit in ((1, dims[axis] - 1), (-1, down)):
                if last is not None and place < last:
                    continue
                if last == place and step != way:
                    continue
                if abs(offset[axis] + step) > limit:
                    continue
                child = list(offset)
                child[axis] += step
                child = tuple(child)
                found.append((child, offset, axis, step, depth + 1))
                frontier.append((child, place, step, depth + 1))
    return found


def product(rows, columns):
    return lax.dot_general(
        rows, columns, (((1,), (1,)), ((), ())), preferred_element_type=F32
    )


def scoped(act):
    def run(*given):
        numbers = [str(g) for g in given if isinstance(g, int)]
        with jax.named_scope("_".join([act.__name__] + numbers)):
            return act(*given)

    return run


class Group:
    def __init__(self, full, halved, place):
        self.full, self.halved = full, halved
        self.dims = tuple(d // 2 if k == halved else d for k, d in enumerate(full))
        self.place = tuple(p // 2 if k == halved else p for k, p in enumerate(place))
        self.parity = lax.rem(place[halved], 2)
        self.size = self.dims[0] * self.dims[1] * self.dims[2]

    def at(self, offset):
        return [
            lax.rem(self.place[k] + offset[k] + self.dims[k], self.dims[k]) for k in range(3)
        ]

    def index(self, offset):
        at = self.at(offset)
        return (at[0] * self.dims[1] + at[1]) * self.dims[2] + at[2]

    def device(self, offset):
        at = self.at(offset)
        at[self.halved] = 2 * at[self.halved] + self.parity
        return (at[0] * self.full[1] + at[1]) * self.full[2] + at[2]

    def neighbour(self, axis, step):
        return self.device(tuple(step if k == axis else 0 for k in range(3)))

    def slot(self, offset):
        at = [offset[k] % self.dims[k] for k in range(3)]
        return (at[0] * self.dims[1] + at[1]) * self.dims[2] + at[2]

    def within(self, pairs):
        holds = None
        for axis, step in sorted(set(pairs)):
            if self.dims[axis] == 2 or step == 0:
                continue
            at = self.place[axis] + step
            one = (at >= 0) if step < 0 else (at < self.dims[axis])
            holds = one if holds is None else jnp.logical_and(holds, one)
        return holds

    def near(self):
        found = [(axis, 1) for axis in range(3) if self.dims[axis] > 1]
        return found + [(axis, -1) for axis in range(3) if self.dims[axis] > 2]


def guarded(holds, act):
    if holds is None:
        act()
    else:
        pl.when(holds)(act)


def of(step, size):
    if isinstance(step, int):
        return pl.ds(step * size, size)
    return pl.ds(pl.multiple_of(step * size, size), size)


def rows(r):
    return of(r, ROWS)


def to(where, src, dst, send, recv):
    return pltpu.make_async_remote_copy(
        src_ref=src,
        dst_ref=dst,
        send_sem=send,
        recv_sem=recv,
        device_id=where,
        device_id_type=MESH,
    )


ORDERS = [
    (0, (Z, X, Y)),
    (0, (Z, X, Y)),
    (0, (Z, X, Y)),
    (0, (Z, X, Y)),
    (1, (Z, Y, X)),
    (1, (Z, Y, X)),
    (1, (Z, Y, X)),
    (1, (Z, Y, X)),
]
ORDER = ";".join(
    [
        "launch 0 1",
        "launch 1 0",
        "launch 0 0",
        "d_cross",
        "launch 1 1",
        "m_cross",
        "m_wait",
        "launch 2 1",
        "launch 3 0",
        "launch 3 1",
        "seq",
        "relay 0 1",
        "launch 5 2",
        "relay 3 1",
        "relay 1 1",
        "relay 3 2",
        "launch 5 0",
        "launch 4 2",
        "norm 0",
        "pass_seq 0",
        "pass_seq 1",
        "relay 3 3",
        "pass_seq 2",
        "d_wait",
        "relay 1 2",
        "relay 1 3",
        "seq_wait",
        "launch 2 0",
        "relay 5 1",
        "relay 5 2",
        "finish 3",
        "launch 6 2",
        "relay 0 2",
        "launch 7 2",
        "launch 4 0",
        "relay 0 3",
        "finish 1",
        "project 1 0",
        "relay 5 3",
        "relay 2 1",
        "relay 4 1",
        "relay 2 2",
        "norm 1",
        "finish 0",
        "project 0 1",
        "relay 4 2",
        "relay 2 3",
        "finish 2",
        "launch 7 0",
        "launch 6 0",
        "project 1 1",
        "relay 4 3",
        "scales",
        "project 0 0",
        "mix_terms 1",
        "finish 5",
        "mix_cross",
        "relay 6 1",
        "mix_terms 0",
        "mix_after 0",
        "mix_after 1",
        "relay 7 1",
        "relay 7 2",
        "relay 7 3",
        "finish 4",
        "relay 6 2",
        "feed 0 0",
        "pass_on 0",
        "feed 0 1",
        "feed 1 0",
        "mix_after 2",
        "feed 0 2",
        "pass_on 1",
        "E 0",
        "feed 1 1",
        "pass_on 2",
        "relay 6 3",
        "E 1",
        "feed 1 2",
        "E 2",
        "L 0",
        "L 1",
        "L 2",
        "Z 0",
        "Z 1",
        "end",
    ]
)


def layer_kernel(
    full,
    seq,
    p_in,
    m_in,
    g_in,
    d_in,
    chan,
    gains,
    hid,
    out,
    pbuf,
    mbuf,
    gbuf,
    dbuf,
    both,
    aft,
    nbuf,
    gated,
    ext,
    hbuf,
    sbuf,
    dsend,
    drecv,
    xsend,
    xrecv,
    frecv,
    w_send,
    w_recv,
    own_sem,
    s_send,
    s_recv,
    x_send,
    x_recv,
    c_send,
    c_recv,
    d_send,
    d_recv,
    y_send,
    y_recv,
):
    me = lax.axis_index("fs")
    core = lax.axis_index("tp")
    peer = {"tp": 1 - core}
    here = (me // (full[1] * full[2]), lax.rem(me // full[2], full[1]), lax.rem(me, full[2]))
    mixer, feeder = Group(full, X, here), Group(full, Y, here)
    groups = (mixer, feeder)
    xp, yp = mixer.parity, feeder.parity
    beside = {"fs": me + 1 - 2 * xp}
    across = {"fs": me + (1 - 2 * yp) * full[2]}
    members = mixer.size
    length, width = seq.shape
    chunks = length // ROWS
    kch = p_in.shape[2]
    fch = g_in.shape[1]
    cols = m_in.shape[1] - 16
    pair = 2 * cols
    span = full[2] * cols
    wide = kch * members
    hidden = fch * members
    origin = (0, 0, 0)
    cut = (pair + 32) // 2 // 16 * 16
    views = [
        lambda i: pbuf.at[0, :, of(i, kch)],
        lambda i: pbuf.at[1, :, of(i, kch)],
        lambda i: mbuf.at[i, pl.ds(0, cut)],
        lambda i: mbuf.at[i, pl.ds(cut, pair + 32 - cut)],
        lambda i: gbuf.at[0, of(i, fch)],
        lambda i: gbuf.at[1, of(i, fch)],
        lambda i: dbuf.at[0, of(i, cols)],
        lambda i: dbuf.at[1, of(i, cols)],
    ]
    inputs = {0: p_in.at[0], 1: p_in.at[1], 4: g_in.at[0], 5: g_in.at[1]}
    plans = [routes(groups[g].dims, order) for g, order in ORDERS]
    base = [sum(len(p) for p in plans[:k]) for k in range(len(plans))]
    deepest = [max(item[4] for item in p) for p in plans]
    arrived = [set() for _ in plans]
    sent = []

    def copy_of(part, number):
        group = groups[ORDERS[part][0]]
        child, parent, axis, step, _ = plans[part][number]
        home = views[part](group.index(parent))
        return to(
            {"fs": group.neighbour(axis, -step)},
            inputs[part] if parent == origin and part in inputs else home,
            home,
            w_send.at[base[part] + number],
            w_recv.at[part, group.slot(child)],
        )

    def launch(part, only=None, parent=origin):
        group = groups[ORDERS[part][0]]
        for number, item in enumerate(plans[part]):
            if item[1] == parent and only in (None, item[2]):
                holds = group.within(list(enumerate(parent)) + [(item[2], -item[3])])
                guarded(holds, copy_of(part, number).start)
                sent.append((part, number, holds))

    def arrive(part, child):
        if child in arrived[part] or child == origin:
            return
        arrived[part].add(child)
        group = groups[ORDERS[part][0]]
        block = views[part](group.index(child))
        there = to(
            peer, block, block, w_send.at[0], w_recv.at[part, group.slot(child)]
        )
        guarded(group.within(list(enumerate(child))), there.wait_recv)

    @scoped
    def relay(part, depth):
        for number, item in enumerate(plans[part]):
            parent = item[1]
            if item[4] == depth + 1 and all(p[1] != parent for p in plans[part][:number]):
                arrive(part, parent)
                launch(part, None, parent)

    @scoped
    def finish(part):
        for item in plans[part]:
            arrive(part, item[0])

    barrier = pltpu.get_barrier_semaphore()
    greeted = [{"fs": g.neighbour(*hop)} for g in groups for hop in g.near()]
    greeted += [beside, across, peer]
    for device in greeted:
        pl.semaphore_signal(barrier, inc=1, device_id=device, device_id_type=MESH)
    pl.semaphore_wait(barrier, len(greeted))

    mine = of(core, width)

    seq_local = pltpu.make_async_copy(seq, both.at[0, :, mine], own_sem.at[0])
    seq_peer = to(peer, seq, both.at[0, :, mine], s_send.at[0], s_recv.at[0])
    seq_beside, seq_pass = [], []
    for r in range(chunks):
        home = both.at[1, rows(r), mine]
        seq_beside.append(
            to(beside, seq.at[rows(r)], home, s_send.at[1 + r], s_recv.at[1 + r])
        )
        at = 1 + chunks + r
        seq_pass.append(to(peer, home, home, s_send.at[at], s_recv.at[at]))
    side = of(xp, cols)
    ends = pl.ds(pl.multiple_of(pair + xp * 16, 16), 16)
    at = 1 + 2 * chunks
    m_home = mbuf.at[mixer.index(origin), side]
    e_home = mbuf.at[mixer.index(origin), ends]
    d_home = dbuf.at[yp, of(feeder.index(origin), cols)]
    body_, end_ = pl.ds(0, cols), pl.ds(cols, 16)
    m_cross = [
        to(beside, m_in.at[1 - xp, body_], m_home, s_send.at[at], s_recv.at[at]),
        to(beside, m_in.at[1 - xp, end_], e_home, s_send.at[at + 1], s_recv.at[at + 1]),
    ]
    d_cross = to(across, d_in.at[1 - yp], d_home, s_send.at[at + 2], s_recv.at[at + 2])
    d_there = dbuf.at[1 - yp, of(feeder.index(origin), cols)]
    d_landed = to(across, d_there, d_there, s_send.at[at + 2], s_recv.at[at + 2])
    m_there = [
        mbuf.at[mixer.index(origin), of(1 - xp, cols)],
        mbuf.at[
            mixer.index(origin), pl.ds(pl.multiple_of(pair + (1 - xp) * 16, 16), 16)
        ],
    ]
    m_landed = [
        to(beside, ref, ref, s_send.at[at + k], s_recv.at[at + k])
        for k, ref in enumerate(m_there)
    ]
    own = [
        pltpu.make_async_copy(m_in.at[xp, body_], m_home, own_sem.at[1]),
        pltpu.make_async_copy(m_in.at[xp, end_], e_home, own_sem.at[2]),
        pltpu.make_async_copy(d_in.at[yp], d_home, own_sem.at[3]),
    ]
    for k, part in enumerate(sorted(inputs)):
        home = views[part](groups[ORDERS[part][0]].index(origin))
        own.append(pltpu.make_async_copy(inputs[part], home, own_sem.at[4 + k]))

    @scoped
    def norm(source, target, first, count, gain):
        tall, deep = 16, 4

        def step(i, _):
            spots = [
                pl.ds(pl.multiple_of(first + (i * deep + k) * tall, tall), tall)
                for k in range(deep)
            ]
            factors = []
            for spot in spots:
                values = source[spot, :].astype(F32)
                mean = jnp.mean(values * values, axis=-1, keepdims=True)
                factors.append(lax.rsqrt(mean + eps))
            for spot, factor in zip(spots, factors):
                scaled = source[spot, :].astype(F32) * factor
                nbuf[target, spot, :] = (scaled * gains[pl.ds(gain, 1), :]).astype(BF16)
            return 0

        lax.fori_loop(0, count // (tall * deep), step, 0)

    def each(act):
        def step(r, _):
            act(r)
            return 0

        lax.fori_loop(0, chunks, step, 0)

    @scoped
    def project(k, s):
        ext[0:8, :] = jnp.zeros((8, wide), F32)

        def act(r):
            block = nbuf[s, rows(r), :]
            inner = product(block, pbuf[k, 1]) * chan[k, 1:2, :]
            value = product(block, pbuf[k, 2]) * chan[k, 2:3, :]
            carried = inner * value
            ext[8 : 8 + ROWS, :] = carried
            conv = chan[k, 3:4, :] * ext[6 : 6 + ROWS, :]
            conv = conv + chan[k, 4:5, :] * ext[7 : 7 + ROWS, :]
            conv = conv + chan[k, 5:6, :] * carried
            ext[0:8, :] = ext[ROWS : ROWS + 8, :]
            outer = product(block, pbuf[k, 0]) * chan[k, 0:1, :]
            gated[s, rows(r), pl.ds(k * wide, wide)] = (outer * conv).astype(BF16)

        each(act)

    @scoped
    def scales():
        def step(g, _):
            tiles = [
                mbuf[g, pl.ds(pair + 16 * e, 16), pl.ds(0, pair)].astype(F32)
                for e in range(2)
            ]
            for which in range(2):
                scale = jnp.zeros((1, pair), F32)
                for tile in tiles:
                    for k in range(3):
                        scale = scale + tile[3 * which + k : 3 * which + k + 1]
                sbuf[which : which + 1, of(g, pair)] = scale
            return 0

        lax.fori_loop(0, members, step, 0)

    def exchange(s, r):
        at = s * chunks + r
        home = drecv.at[s, rows(r)]
        return to(peer, dsend.at[s, rows(r)], home, c_send.at[at], c_recv.at[at])

    def crossing(r):
        return to(beside, xsend.at[1, rows(r)], xrecv.at[rows(r)], x_send.at[r], x_recv.at[r])

    def spread(r):
        at = 2 * chunks + r
        home = both.at[0, rows(r), mine]
        return to(peer, home, home, c_send.at[at], c_recv.at[at])

    def afar(r):
        at = chunks + r
        return to(
            across, both.at[0, rows(r), mine], aft.at[rows(r), mine], x_send.at[at], x_recv.at[at]
        )

    def onward(r):
        at = 3 * chunks + r
        home = aft.at[rows(r), mine]
        return to(peer, home, home, c_send.at[at], c_recv.at[at])

    half = members // 2

    @scoped
    def mix_terms(s):
        def act(r):
            def away(i, _):
                g = (1 - core) * half + i
                term = product(gated[s, rows(r), :], mbuf[g, pl.ds(0, pair), :])
                dsend[s, rows(r), of(i, pair)] = (term * sbuf[0:1, of(g, pair)]).astype(BF16)
                return 0

            def keep(i, _):
                g = core * half + i
                term = product(gated[s, rows(r), :], mbuf[g, pl.ds(0, pair), :])
                xsend[s, rows(r), of(i, pair)] = (term * sbuf[0:1, of(g, pair)]).astype(BF16)
                return 0

            for i in range(half):
                away(i, 0)
            exchange(s, r).start()
            for i in range(half):
                keep(i, 0)

        each(act)

    @scoped
    def mix_cross():
        def act(r):
            copy = exchange(1, r)
            copy.wait_recv()
            total = xsend[1, rows(r), :].astype(F32) + drecv[1, rows(r), :].astype(F32)
            xsend[1, rows(r), :] = total.astype(BF16)
            crossing(r).start()

        each(act)

    @scoped
    def mix_after(r):
        exchange(0, r).wait_recv()
        crossing(r).wait_recv()
        mix = xsend[0, rows(r), :].astype(F32) + drecv[0, rows(r), :].astype(F32)
        mix = mix + xrecv[rows(r), :].astype(F32)
        after = both[0, rows(r), mine].astype(F32) + mix
        both[0, rows(r), mine] = after.astype(BF16)
        afar(r).start()
        spread(r).start()

    @scoped
    def pass_on(r):
        afar(r).wait_recv()
        onward(r).start()

    @scoped
    def feed(s, r):
        (spread, onward)[s](r).wait_recv()
        norm((both.at[0], aft)[s], s, r * ROWS, ROWS, 1)

        def unit(i, _):
            at = of(i, wide)
            block = nbuf[s, rows(r), :]
            gate = product(block, gbuf[0, at, :]) * hid[0:1, at]
            up = product(block, gbuf[1, at, :]) * hid[1:2, at]
            hbuf[s, rows(r), at] = (gate / (1.0 + jnp.exp(-gate)) * up).astype(BF16)
            return 0

        lax.fori_loop(0, hidden // wide, unit, 0)

    blocks = 2 * feeder.dims[0] * feeder.dims[1]
    held = blocks // 2

    def where(j, spot):
        at = feeder.at(spot)
        return (at[0] * feeder.dims[1] + at[1]) * 2 + j

    def inside(spot, holds=None):
        there = feeder.within(list(enumerate(spot)))
        if there is None or holds is None:
            return holds if there is None else there
        return jnp.logical_and(holds, there)

    def lent(s, b, r):
        at = (s * blocks + b) * chunks + r
        local = of(lax.rem(b, held), span)
        return to(
            peer,
            nbuf.at[s, rows(r), of(b, span)],
            drecv.at[s, rows(r), local],
            d_send.at[at],
            d_recv.at[at],
        )

    def sends(b, r):
        at = b * chunks + r
        local = of(lax.rem(b, held), span)
        return to(
            across,
            nbuf.at[1, rows(r), of(b, span)],
            frecv.at[rows(r), local],
            y_send.at[at],
            y_recv.at[at],
        )

    spots = sorted(
        {(item[0][0], item[0][1], 0) for item in plans[6]} | {origin},
        key=lambda o: (abs(o[0]) + abs(o[1]), o),
    )
    units = [
        [(j, spot) for spot in spots for j in range(2) if (abs(spot[0]) + abs(spot[1]) < 2) == near]
        for near in (True, False)
    ]

    def landed(j, spot):
        for item in plans[6 + j]:
            if item[0][:2] == spot[:2]:
                arrive(6 + j, item[0])

    def term(s, j, spot, r):
        b = where(j, spot)
        value = product(hbuf[s, rows(r), :], dbuf[j, of(b // 2, span), :])
        value = value * sbuf[1:2, of(b, span)]
        nbuf[s, rows(r), of(b, span)] = value.astype(BF16)
        pl.when(b // held != core)(lent(s, b, r).start)

    def settle(j, spot, r):
        b = where(j, spot)

        def run():
            lent(1, b, r).wait_recv()
            theirs = drecv[1, rows(r), of(lax.rem(b, held), span)]
            total = nbuf[1, rows(r), of(b, span)].astype(F32) + theirs.astype(F32)
            nbuf[1, rows(r), of(b, span)] = total.astype(BF16)
            sends(b, r).start()

        pl.when(inside(spot, b // held == core))(run)

    @scoped
    def down(late, r):
        ahead = None
        for j, spot in units[late]:
            landed(j, spot)
            guarded(inside(spot), functools.partial(term, 1, j, spot, r))
            if ahead:
                settle(*ahead, r)
            ahead = (j, spot)
        if ahead:
            settle(*ahead, r)

    @scoped
    def down_own(late):
        for j, spot in units[late]:
            landed(j, spot)
            guarded(inside(spot), lambda: each(functools.partial(term, 0, j, spot)))

    def close(j, spot):
        b = where(j, spot)
        local = of(lax.rem(b, held), span)

        def act(r):
            lent(0, b, r).wait_recv()
            sends(b, r).wait_recv()
            ffn = nbuf[0, rows(r), of(b, span)].astype(F32)
            ffn = ffn + drecv[0, rows(r), local].astype(F32)
            ffn = ffn + frecv[rows(r), local].astype(F32)
            after = both[0, rows(r), of(b, span)].astype(F32)
            out[rows(r), local] = (after + ffn).astype(BF16)

        pl.when(inside(spot, b // held == core))(lambda: each(act))

    @scoped
    def end():
        for j, spot in units[0] + units[1]:
            close(j, spot)

    @scoped
    def seq_start():
        for copy in seq_beside:
            copy.start()

    @scoped
    def m_cross_start():
        for copy in m_cross:
            copy.start()

    @scoped
    def m_wait():
        for copy in own[:2]:
            copy.wait()
        for copy in m_landed:
            copy.wait_recv()

    @scoped
    def d_wait():
        own[2].wait()
        d_landed.wait_recv()

    @scoped
    def pass_seq(r):
        seq_beside[r].wait_recv()
        seq_pass[r].start()

    @scoped
    def seq_wait():
        for copy in seq_pass:
            copy.wait()

    def norm_of(s):
        if s == 0:
            seq_local.wait()
            seq_peer.wait_recv()
        norm(both.at[s], s, 0, length, 0)

    def finished(part):
        finish(part)
        if part in inputs:
            own[3 + sorted(inputs).index(part)].wait()

    def relays(part, depth):
        if depth < deepest[part]:
            relay(part, depth)

    acts = {
        "launch": launch,
        "relay": relays,
        "finish": finished,
        "seq": seq_start,
        "m_cross": m_cross_start,
        "m_wait": m_wait,
        "d_cross": lambda: d_cross.start(),
        "d_wait": d_wait,
        "pass_seq": pass_seq,
        "seq_wait": seq_wait,
        "norm": norm_of,
        "project": project,
        "scales": scales,
        "mix_terms": mix_terms,
        "mix_cross": mix_cross,
        "mix_after": mix_after,
        "pass_on": pass_on,
        "feed": feed,
        "E": functools.partial(down, 0),
        "L": functools.partial(down, 1),
        "Z": down_own,
        "end": end,
    }
    seq_peer.start()
    seq_local.start()
    for copy in own:
        copy.start()
    extra = max(deepest) - 1
    for line in ORDER.split(";"):
        name, *given = line.split()
        given = [int(g) for g in given]
        acts[name](*given)
        if name == "relay" and given[1] == 3:
            for depth in range(4, extra + 1):
                relays(given[0], depth)
    for part, number, holds in sent:
        guarded(holds, copy_of(part, number).wait_send)
    seq_peer.wait_send()
    d_cross.wait_send()
    for copy in seq_beside + m_cross:
        copy.wait_send()

    def drain(r):
        crossing(r).wait_send()
        for s in range(2):
            exchange(s, r).wait_send()
        spread(r).wait_send()
        afar(r).wait_send()
        onward(r).wait_send()
        for k in range(held):
            sends(core * held + k, r).wait_send()
            for s in range(2):
                lent(s, (1 - core) * held + k, r).wait_send()

    each(drain)


def prepare(
    full,
    proj_outer,
    proj_inner,
    proj_value,
    proj_scales,
    taps,
    mix_out,
    mix_out_scale,
    ffn_gate,
    ffn_up,
    ffn_scales,
    ffn_down,
    down_scale,
):
    half = full[0] * full[1] * full[2] // 2
    lines, columns = half // full[2], full[2]
    me = lax.axis_index("fs")
    xp, yp = lax.rem(me, 2), lax.rem(me // columns, 2)
    each = proj_outer.shape[1]
    kch = each // 2
    p_in = jnp.stack(
        [w.astype(BF16).T.reshape(2, kch, -1) for w in (proj_outer, proj_inner, proj_value)],
        axis=1,
    )
    units = ffn_gate.shape[1]
    fill = -units % 16
    g_in = jnp.stack(
        [jnp.pad(w.astype(BF16).T, ((0, fill), (0, 0))) for w in (ffn_gate, ffn_up)]
    )
    cols = mix_out.shape[1]
    mixed = mix_out.astype(BF16).T.reshape(cols, half, 2, 2, kch)
    mixed = mixed.transpose(2, 0, 3, 1, 4).reshape(2, cols, half * each)
    thin = []
    for scale in (mix_out_scale, down_scale):
        high = lax.reduce_precision(scale, 8, 7)
        middle = lax.reduce_precision(scale - high, 8, 7)
        thin += [high, middle, scale - high - middle]
    thin = jnp.stack(thin)
    ours = (lax.iota(jnp.int32, 2 * cols) // cols == xp)[None]
    thin = jnp.where(ours, jnp.concatenate([thin, thin], 1), 0.0).astype(BF16)
    thin = jnp.pad(thin, ((0, 10), (0, half * each - 2 * cols)))
    m_in = jnp.concatenate([mixed, jnp.broadcast_to(thin, (2,) + thin.shape)], axis=1)
    down = ffn_down.astype(BF16).T.reshape(cols, lines, 2, columns, units)
    down = jnp.pad(down, ((0, 0), (0, 0), (0, 0), (0, 0), (0, fill)))
    d_in = down.transpose(2, 0, 1, 3, 4).reshape(2, cols, -1)
    chan = jnp.concatenate([proj_scales, taps]).reshape(6, half, 2, 2, kch)
    chan = lax.dynamic_index_in_dim(chan, xp, 2, keepdims=False)
    chan = chan.transpose(2, 0, 1, 3).reshape(2, 6, half * kch)
    chan = jnp.pad(chan, ((0, 0), (0, 2), (0, 0)))
    hid = ffn_scales.reshape(2, lines, 2, columns, units)
    hid = lax.dynamic_index_in_dim(hid, yp, 2, keepdims=False)
    hid = jnp.pad(hid, ((0, 6), (0, 0), (0, 0), (0, fill))).reshape(8, -1)
    return p_in, m_in, g_in, d_in, chan, hid


def body(n, sequence, mix_gain, ffn_gain, *rest):
    seq = sequence[0]
    length, width = seq.shape
    depth = 2 * width
    full = grid_of(n)
    p_in, m_in, g_in, d_in, chan, hid = prepare(full, *rest)
    gains = jnp.pad(jnp.stack([mix_gain, ffn_gain]), ((0, 6), (0, 0)))
    members = n // 2
    kch, fch = p_in.shape[2], g_in.shape[1]
    cols = m_in.shape[1] - 16
    chunks = length // ROWS
    units = members * fch
    items = len(ORDERS) * 4 * members
    operands = (seq, p_in, m_in, g_in, d_in, chan, gains, hid)
    sems = [pltpu.SemaphoreType.DMA((k,)) for k in (items,)]
    sems += [pltpu.SemaphoreType.DMA((len(ORDERS), members)), pltpu.SemaphoreType.DMA((8,))]
    for k in (4 + 2 * chunks, 2 * chunks, 4 * chunks, 2 * n * chunks, n * chunks):
        sems += [pltpu.SemaphoreType.DMA((k,))] * 2
    result = pl.pallas_call(
        functools.partial(layer_kernel, full),
        out_shape=jax.ShapeDtypeStruct(seq.shape, BF16),
        in_specs=[pl.BlockSpec(memory_space=pltpu.VMEM)] * len(operands),
        out_specs=pl.BlockSpec(memory_space=pltpu.VMEM),
        scratch_shapes=[
            pltpu.VMEM((2, 3, members * kch, depth), BF16),
            pltpu.VMEM((members, 2 * cols + 32, m_in.shape[2]), BF16),
            pltpu.VMEM((2, units, depth), BF16),
            pltpu.VMEM((2, members * cols, units), BF16),
            pltpu.VMEM((2, length, depth), BF16),
            pltpu.VMEM((length, depth), BF16),
            pltpu.VMEM((2, length, depth), BF16),
            pltpu.VMEM((2, length, m_in.shape[2]), BF16),
            pltpu.VMEM((8 + ROWS, members * kch), F32),
            pltpu.VMEM((2, length, units), BF16),
            pltpu.VMEM((8, depth), F32),
            pltpu.VMEM((2, length, width), BF16),
            pltpu.VMEM((2, length, width), BF16),
            pltpu.VMEM((2, length, width), BF16),
            pltpu.VMEM((length, width), BF16),
            pltpu.VMEM((length, width), BF16),
        ]
        + sems,
        compiler_params=pltpu.CompilerParams(
            collective_id=0, has_side_effects=True, vmem_limit_bytes=67043328
        ),
        name="layer",
    )(*operands)
    return result[None]


def solution(mesh):
    in_specs = (
        P(("rep", "fs"), None, "tp"),
        P(),
        P(),
        P(None, ("tp", "fs")),
        P(None, ("tp", "fs")),
        P(None, ("tp", "fs")),
        P(None, "tp"),
        P(None, "tp"),
        P("tp", "fs"),
        P("fs"),
        P(None, ("tp", "fs")),
        P(None, ("tp", "fs")),
        P(None, "tp"),
        P("tp", "fs"),
        P("fs"),
    )
    out_specs = P(("rep", "fs"), None, "tp")
    return jax.shard_map(
        functools.partial(body, mesh.shape["fs"]),
        mesh=mesh,
        in_specs=in_specs,
        out_specs=out_specs,
        check_vma=False,
    )
```

time: 276 us -> 240 us (0.87)
  the two profiles are of different devices: /device:TPU:0 before, /device:TPU:1 now
where the time goes in v1:
time: 240 us; the launch traced here: 239 us
  Pallas kernels  226 us (94%)
  local copies, waits for them, and re-layouts  6.88 us (3%)
  other arithmetic  6.84 us (3%)
    pallas_call x1, Pallas kernels, body(): pl.pallas_call(functools.partial(layer_kernel, full), out_shape=jax.Shape...  226 us

profile of v1, /device:TPU:1, one launch (start us, length us, event | category | flops | bytes accessed | tf_op | source)
XLA Modules:
  0.0 239.4 jit_solution(15818854267335995850)
XLA Ops:
  0.0 0.8 fusion.2
  0.8 0.8 reshape.44
  1.7 0.7 reshape.45.hid
  2.4 0.7 pad_maximum_fusion.3
  3.1 0.1 reshape.42
  3.3 0.1 reshape.43
  3.4 0.6 pad.31.chan
  4.0 1.4 select_maximum_fusion.gains
  5.4 1.1 convert_element_type.37
  6.5 0.0 copy-done.3
  6.5 0.0 copy-start.5
  6.6 1.0 pad_maximum_fusion.p_in
  7.5 0.0 copy-done.5
  7.6 0.1 copy.24
  7.7 0.8 pad_maximum_fusion.2.m_in
  8.5 0.1 copy-done
  8.7 0.3 copy-done.1
  9.0 0.0 copy-start.2
  9.0 0.1 pad_bitcast_fusion.1
  9.1 1.0 pad_maximum_fusion.1.g_in
  10.1 0.1 copy-done.2
  10.3 0.9 copy.28.d_in
  11.2 225.5 %layer.1 = bf16[768,1024]{1,0:T(8,128)(2,1)} custom-call(bf16[768,1024]{1,0:T(8,128)(2,1)} %bitcast.58, bf16[2,3,32,2048]{3,2,1,0:T(8,128)(2,1)} %pad_maximum_fusion.p_in, bf16[2,144,512]{2,1,0:T(8,128)(2,1)} %pad_maximum_fusion.2.m_in, bf16[2,96,2048]{2,1,0:T(8,128)(2,1)} %pad_maximum_fusion.1.g_in, bf16[2,128,768]{2,1,0:T(8,128)(2,1)} %copy.28.d_in, ...), custom_call_target="tpu_custom_call" | custom-call | tf_op jit(solution)/shard_map/layer/pallas_call | solution.py:852
  236.7 2.7 %copy.32 = bf16[1,768,1024]{2,1,0:T(8,128)(2,1)} copy(bf16[1,768,1024]{2,1,0:T(8,128)(2,1)} %bitcast.56) | data formatting | bytes 3145728
  (24 shorter events, 0.4 us)
Async XLA Ops:
  0.0 6.5 %copy-start.4 = (f32[2048,64]{0,1:T(8,128)S(1)}, f32[2048,64]{0,1:T(8,128)}, u32[]{:S(2)}) copy-start(f32[2048,64]{0,1:T(8,128)} %param.20) | copy-start | bytes 1572868
  0.0 6.5 %copy-start.3 = (f32[2048,64]{0,1:T(8,128)S(1)}, f32[2048,64]{0,1:T(8,128)}, u32[]{:S(2)}) copy-start(f32[2048,64]{0,1:T(8,128)} %param.19) | copy-start | bytes 1572868
  6.5 1.1 copy-start.5
  7.5 1.1 copy-start
  7.5 1.4 copy-start.1
  9.0 1.2 copy-start.2

commit v2 on v1

--- a/solution.py
+++ b/solution.py
@@ -139,110 +139,54 @@
     (0, (Z, X, Y)),
     (1, (Z, Y, X)),
     (1, (Z, Y, X)),
-    (1, (Z, Y, X)),
-    (1, (Z, Y, X)),
+    (1, (X, Y, Z)),
+    (1, (X, Y, Z)),
 ]
-ORDER = ";".join(
-    [
-        "launch 0 1",
-        "launch 1 0",
-        "launch 0 0",
-        "d_cross",
-        "launch 1 1",
-        "m_cross",
-        "m_wait",
-        "launch 2 1",
-        "launch 3 0",
-        "launch 3 1",
-        "seq",
-        "relay 0 1",
-        "launch 5 2",
-        "relay 3 1",
-        "relay 1 1",
-        "relay 3 2",
-        "launch 5 0",
-        "launch 4 2",
-        "norm 0",
-        "pass_seq 0",
-        "pass_seq 1",
-        "relay 3 3",
-        "pass_seq 2",
-        "d_wait",
-        "relay 1 2",
-        "relay 1 3",
-        "seq_wait",
-        "launch 2 0",
-        "relay 5 1",
-        "relay 5 2",
-        "finish 3",
-        "launch 6 2",
-        "relay 0 2",
-        "launch 7 2",
-        "launch 4 0",
-        "relay 0 3",
-        "finish 1",
-        "project 1 0",
-        "relay 5 3",
-        "relay 2 1",
-        "relay 4 1",
-        "relay 2 2",
-        "norm 1",
-        "finish 0",
-        "project 0 1",
-        "relay 4 2",
-        "relay 2 3",
-        "finish 2",
-        "launch 7 0",
-        "launch 6 0",
-        "project 1 1",
-        "relay 4 3",
-        "scales",
-        "project 0 0",
-        "mix_terms 1",
-        "finish 5",
-        "mix_cross",
-        "relay 6 1",
-        "mix_terms 0",
-        "mix_after 0",
-        "mix_after 1",
-        "relay 7 1",
-        "relay 7 2",
-        "relay 7 3",
-        "finish 4",
-        "relay 6 2",
-        "feed 0 0",
-        "pass_on 0",
-        "feed 0 1",
-        "feed 1 0",
-        "mix_after 2",
-        "feed 0 2",
-        "pass_on 1",
-        "E 0",
-        "feed 1 1",
-        "pass_on 2",
-        "relay 6 3",
-        "E 1",
-        "feed 1 2",
-        "E 2",
-        "L 0",
-        "L 1",
-        "L 2",
-        "Z 0",
-        "Z 1",
-        "end",
-    ]
+(
+    LAUNCH, RELAY, FINISH, ROWS_SWAP, MIX_SWAP, MIX_WAIT, DOWN_SWAP, DOWN_WAIT, ROWS_PASS,
+    ROWS_WAIT, NORM, PROJECT, SCALES, MIX_AWAY, MIX_OWN, MIX_SEND, MIX_AFTER, AFTER_PASS, FEED_UP,
+    FEED_GATE, DOWN_NEAR, DOWN_FAR, DOWN_OWN, END,
+) = range(24)
+
+ORDER = (
+    (LAUNCH, 1, 0), (LAUNCH, 1, 1), (MIX_SWAP,), (DOWN_SWAP,), (LAUNCH, 5, 2), (NORM, 0), (MIX_WAIT,),
+    (LAUNCH, 3, 0), (RELAY, 1, 0), (RELAY, 1, 1), (LAUNCH, 0, 0), (LAUNCH, 4, 2), (RELAY, 1, 3),
+    (LAUNCH, 3, 1), (DOWN_WAIT,), (RELAY, 1, 2), (RELAY, 3, 1), (ROWS_SWAP,), (RELAY, 3, 0),
+    (RELAY, 1, 4), (RELAY, 3, 2), (RELAY, 3, 4), (LAUNCH, 2, 0), (RELAY, 2, 0), (LAUNCH, 6, 2), (RELAY, 1, 5),
+    (RELAY, 3, 3), (RELAY, 3, 5), (LAUNCH, 5, 0), (RELAY, 0, 1), (LAUNCH, 7, 2), (FINISH, 1),
+    (PROJECT, 1, 0), (RELAY, 0, 0), (RELAY, 2, 1), (FINISH, 3), (RELAY, 5, 1), (ROWS_PASS, 0),
+    (ROWS_PASS, 1), (RELAY, 5, 0), (LAUNCH, 0, 1), (RELAY, 2, 3), (RELAY, 0, 3), (RELAY, 0, 2),
+    (LAUNCH, 4, 0), (RELAY, 0, 4), (ROWS_PASS, 2), (RELAY, 2, 5), (ROWS_WAIT,), (RELAY, 2, 2),
+    (RELAY, 5, 2), (NORM, 1), (RELAY, 5, 3), (RELAY, 0, 5), (RELAY, 4, 1), (LAUNCH, 2, 1), (PROJECT, 1, 1),
+    (RELAY, 5, 5), (RELAY, 2, 4), (RELAY, 4, 0), (FINISH, 0), (PROJECT, 0, 1), (RELAY, 5, 4), (FINISH, 2),
+    (SCALES,), (RELAY, 6, 0), (LAUNCH, 6, 0), (MIX_AWAY, 0), (MIX_AWAY, 1), (MIX_AWAY, 2),
+    (MIX_SEND, 0), (MIX_SEND, 1), (LAUNCH, 7, 0), (MIX_SEND, 2), (PROJECT, 0, 0), (MIX_OWN, 0),
+    (RELAY, 4, 3), (MIX_OWN, 2), (RELAY, 6, 3), (MIX_OWN, 1), (MIX_AFTER, 0), (RELAY, 6, 4),
+    (MIX_AFTER, 1), (RELAY, 7, 0), (RELAY, 7, 1), (FINISH, 5), (FEED_UP, 0, 1), (FEED_UP, 0, 0),
+    (RELAY, 4, 2), (RELAY, 4, 4), (RELAY, 4, 5), (MIX_AFTER, 2), (RELAY, 7, 3), (RELAY, 6, 1), (RELAY, 7, 4),
+    (FEED_UP, 0, 2), (AFTER_PASS, 0), (AFTER_PASS, 1), (RELAY, 7, 2), (FEED_UP, 1, 0), (RELAY, 6, 2),
+    (FEED_UP, 1, 1), (RELAY, 7, 7), (FINISH, 4), (FEED_GATE, 1, 0), (RELAY, 6, 8), (AFTER_PASS, 2),
+    (RELAY, 7, 5), (RELAY, 7, 6), (DOWN_NEAR, 0), (RELAY, 6, 5), (FEED_GATE, 1, 1), (DOWN_NEAR, 1),
+    (RELAY, 7, 8), (FEED_UP, 1, 2), (FEED_GATE, 1, 2), (RELAY, 6, 7), (RELAY, 6, 6), (DOWN_FAR, 0),
+    (DOWN_FAR, 1), (FEED_GATE, 0, 0), (FEED_GATE, 0, 1), (DOWN_NEAR, 2), (DOWN_FAR, 2),
+    (FEED_GATE, 0, 2), (DOWN_OWN, 0), (DOWN_OWN, 1), (END,),
 )
 
 
 def layer_kernel(
     full,
     seq,
-    p_in,
+    po_in,
+    pi_in,
+    pv_in,
     m_in,
-    g_in,
+    gate_in,
+    up_in,
     d_in,
+    thin,
     chan,
-    gains,
+    mix_gain,
+    ffn_gain,
     hid,
     out,
     pbuf,
@@ -256,6 +200,10 @@
     ext,
     hbuf,
     sbuf,
+    m_out,
+    d_out,
+    m_tmp,
+    d_tmp,
     dsend,
     drecv,
     xsend,
@@ -287,9 +235,11 @@
     members = mixer.size
     length, width = seq.shape
     chunks = length // ROWS
-    kch = p_in.shape[2]
-    fch = g_in.shape[1]
-    cols = m_in.shape[1] - 16
+    kch = po_in.shape[0] // 2
+    units_in = gate_in.shape[0]
+    units_sent = units_in + -units_in % 8
+    fch = gbuf.shape[1] // members
+    cols = m_in.shape[1]
     pair = 2 * cols
     span = full[2] * cols
     wide = kch * members
@@ -301,12 +251,11 @@
         lambda i: pbuf.at[1, :, of(i, kch)],
         lambda i: mbuf.at[i, pl.ds(0, cut)],
         lambda i: mbuf.at[i, pl.ds(cut, pair + 32 - cut)],
-        lambda i: gbuf.at[0, of(i, fch)],
-        lambda i: gbuf.at[1, of(i, fch)],
+        lambda i: gbuf.at[0, pl.ds(pl.multiple_of(i * fch, 16), units_sent)],
+        lambda i: gbuf.at[1, pl.ds(pl.multiple_of(i * fch, 16), units_sent)],
         lambda i: dbuf.at[0, of(i, cols)],
         lambda i: dbuf.at[1, of(i, cols)],
     ]
-    inputs = {0: p_in.at[0], 1: p_in.at[1], 4: g_in.at[0], 5: g_in.at[1]}
     plans = [routes(groups[g].dims, order) for g, order in ORDERS]
     base = [sum(len(p) for p in plans[:k]) for k in range(len(plans))]
     deepest = [max(item[4] for item in p) for p in plans]
@@ -319,7 +268,7 @@
         home = views[part](group.index(parent))
         return to(
             {"fs": group.neighbour(axis, -step)},
-            inputs[part] if parent == origin and part in inputs else home,
+            home,
             home,
             w_send.at[base[part] + number],
             w_recv.at[part, group.slot(child)],
@@ -344,18 +293,29 @@
         )
         guarded(group.within(list(enumerate(child))), there.wait_recv)
 
-    @scoped
-    def relay(part, depth):
-        for number, item in enumerate(plans[part]):
-            parent = item[1]
-            if item[4] == depth + 1 and all(p[1] != parent for p in plans[part][:number]):
-                arrive(part, parent)
-                launch(part, None, parent)
+    forks = []
+    for plan in plans:
+        found = []
+        for item in sorted(plan, key=lambda item: item[4]):
+            if item[1] != origin and item[1] not in found:
+                found.append(item[1])
+        forks.append(found)
+
+    @scoped
+    def relay(part, number):
+        arrive(part, forks[part][number])
+        launch(part, None, forks[part][number])
 
     @scoped
     def finish(part):
         for item in plans[part]:
             arrive(part, item[0])
+
+    if fch > units_in:
+        for which in range(2):
+            for i in range(members):
+                spot = pl.ds(i * fch + units_in, fch - units_in)
+                gbuf[which, spot, :] = jnp.zeros((fch - units_in, 2 * width), BF16)
 
     barrier = pltpu.get_barrier_semaphore()
     greeted = [{"fs": g.neighbour(*hop)} for g in groups for hop in g.near()]
@@ -382,12 +342,11 @@
     m_home = mbuf.at[mixer.index(origin), side]
     e_home = mbuf.at[mixer.index(origin), ends]
     d_home = dbuf.at[yp, of(feeder.index(origin), cols)]
-    body_, end_ = pl.ds(0, cols), pl.ds(cols, 16)
     m_cross = [
-        to(beside, m_in.at[1 - xp, body_], m_home, s_send.at[at], s_recv.at[at]),
-        to(beside, m_in.at[1 - xp, end_], e_home, s_send.at[at + 1], s_recv.at[at + 1]),
+        to(beside, m_out, m_home, s_send.at[at], s_recv.at[at]),
+        to(beside, thin, e_home, s_send.at[at + 1], s_recv.at[at + 1]),
     ]
-    d_cross = to(across, d_in.at[1 - yp], d_home, s_send.at[at + 2], s_recv.at[at + 2])
+    d_cross = to(across, d_out, d_home, s_send.at[at + 2], s_recv.at[at + 2])
     d_there = dbuf.at[1 - yp, of(feeder.index(origin), cols)]
     d_landed = to(across, d_there, d_there, s_send.at[at + 2], s_recv.at[at + 2])
     m_there = [
@@ -400,17 +359,60 @@
         to(beside, ref, ref, s_send.at[at + k], s_recv.at[at + k])
         for k, ref in enumerate(m_there)
     ]
-    own = [
-        pltpu.make_async_copy(m_in.at[xp, body_], m_home, own_sem.at[1]),
-        pltpu.make_async_copy(m_in.at[xp, end_], e_home, own_sem.at[2]),
-        pltpu.make_async_copy(d_in.at[yp], d_home, own_sem.at[3]),
-    ]
-    for k, part in enumerate(sorted(inputs)):
-        home = views[part](groups[ORDERS[part][0]].index(origin))
-        own.append(pltpu.make_async_copy(inputs[part], home, own_sem.at[4 + k]))
-
-    @scoped
-    def norm(source, target, first, count, gain):
+
+    @scoped
+    def p_ready():
+        spot = of(mixer.index(origin), kch)
+        for k in range(2):
+            for which, ref in enumerate((po_in, pi_in, pv_in)):
+                pbuf[k, which, spot, :] = ref[pl.ds(k * kch, kch), :].astype(BF16)
+
+    @scoped
+    def g_ready():
+        spot = pl.ds(pl.multiple_of(feeder.index(origin) * fch, 16), units_in)
+        for which, ref in enumerate((gate_in, up_in)):
+            gbuf[which, spot, :] = ref[...].astype(BF16)
+
+    @scoped
+    def m_ready():
+        each_in = 2 * kch
+        for target in range(2):
+            to_x = xp if target else 1 - xp
+            for g in range(members):
+                for k in range(2):
+                    source = pl.multiple_of((2 * g + to_x) * each_in + k * kch, kch)
+                    m_tmp[pl.ds(k * wide + g * kch, kch), :] = m_in[pl.ds(source, kch), :]
+            for tile in range(m_tmp.shape[0] // 128):
+                at_ = pl.ds(tile * 128, 128)
+                turned = m_tmp[at_, :].T.astype(BF16)
+                if target:
+                    m_home[:, at_] = turned
+                else:
+                    m_out[:, at_] = turned
+        e_home[...] = thin[...]
+
+    @scoped
+    def d_ready():
+        for target in range(2):
+            to_y = yp if target else 1 - yp
+            for i in range(members):
+                line, x = i // full[2], i % full[2]
+                source = ((2 * line + to_y) * full[2] + x) * units_in
+                spot = pl.ds(i * fch, units_in)
+                d_tmp[spot, :] = d_in[pl.ds(pl.multiple_of(source, 4), units_in), :]
+                if fch > units_in:
+                    fill = fch - units_in
+                    d_tmp[pl.ds(i * fch + units_in, fill), :] = jnp.zeros((fill, cols), F32)
+            for tile in range(d_tmp.shape[0] // 128):
+                at_ = pl.ds(tile * 128, 128)
+                turned = d_tmp[at_, :].T.astype(BF16)
+                if target:
+                    d_home[:, at_] = turned
+                else:
+                    d_out[:, at_] = turned
+
+    @scoped
+    def norm(source, target, first, count, gains):
         tall, deep = 16, 4
 
         def step(i, _):
@@ -425,7 +427,7 @@
                 factors.append(lax.rsqrt(mean + eps))
             for spot, factor in zip(spots, factors):
                 scaled = source[spot, :].astype(F32) * factor
-                nbuf[target, spot, :] = (scaled * gains[pl.ds(gain, 1), :]).astype(BF16)
+                nbuf[target, spot, :] = (scaled * gains[...]).astype(BF16)
             return 0
 
         lax.fori_loop(0, count // (tall * deep), step, 0)
@@ -500,38 +502,23 @@
     half = members // 2
 
     @scoped
-    def mix_terms(s):
-        def act(r):
-            def away(i, _):
-                g = (1 - core) * half + i
-                term = product(gated[s, rows(r), :], mbuf[g, pl.ds(0, pair), :])
-                dsend[s, rows(r), of(i, pair)] = (term * sbuf[0:1, of(g, pair)]).astype(BF16)
-                return 0
-
-            def keep(i, _):
-                g = core * half + i
-                term = product(gated[s, rows(r), :], mbuf[g, pl.ds(0, pair), :])
-                xsend[s, rows(r), of(i, pair)] = (term * sbuf[0:1, of(g, pair)]).astype(BF16)
-                return 0
-
-            for i in range(half):
-                away(i, 0)
-            exchange(s, r).start()
-            for i in range(half):
-                keep(i, 0)
-
-        each(act)
-
-    @scoped
-    def mix_cross():
-        def act(r):
-            copy = exchange(1, r)
-            copy.wait_recv()
-            total = xsend[1, rows(r), :].astype(F32) + drecv[1, rows(r), :].astype(F32)
-            xsend[1, rows(r), :] = total.astype(BF16)
-            crossing(r).start()
-
-        each(act)
+    def mix_terms(s, r):
+        def block(g, ref, i):
+            term = product(gated[s, rows(r), :], mbuf[g, pl.ds(0, pair), :])
+            ref[s, rows(r), of(i, pair)] = (term * sbuf[0:1, of(g, pair)]).astype(BF16)
+
+        for i in range(half):
+            block((1 - core) * half + i, dsend, i)
+        exchange(s, r).start()
+        for i in range(half):
+            block(core * half + i, xsend, i)
+
+    @scoped
+    def mix_cross(r):
+        exchange(1, r).wait_recv()
+        total = xsend[1, rows(r), :].astype(F32) + drecv[1, rows(r), :].astype(F32)
+        xsend[1, rows(r), :] = total.astype(BF16)
+        crossing(r).start()
 
     @scoped
     def mix_after(r):
@@ -549,20 +536,32 @@
         afar(r).wait_recv()
         onward(r).start()
 
+    def wide_steps(act):
+        def step(i, _):
+            act(of(i, wide))
+            return 0
+
+        lax.fori_loop(0, hidden // wide, step, 0)
+
+    @scoped
+    def feed_up(s, r):
+        (spread, onward)[s](r).wait_recv()
+        norm((both.at[0], aft)[s], s, r * ROWS, ROWS, ffn_gain)
+
+        def act(at):
+            up = product(nbuf[s, rows(r), :], gbuf[1, at, :]) * hid[1:2, at]
+            hbuf[s, rows(r), at] = up.astype(BF16)
+
+        wide_steps(act)
+
     @scoped
     def feed(s, r):
-        (spread, onward)[s](r).wait_recv()
-        norm((both.at[0], aft)[s], s, r * ROWS, ROWS, 1)
-
-        def unit(i, _):
-            at = of(i, wide)
-            block = nbuf[s, rows(r), :]
-            gate = product(block, gbuf[0, at, :]) * hid[0:1, at]
-            up = product(block, gbuf[1, at, :]) * hid[1:2, at]
+        def act(at):
+            gate = product(nbuf[s, rows(r), :], gbuf[0, at, :]) * hid[0:1, at]
+            up = hbuf[s, rows(r), at].astype(F32)
             hbuf[s, rows(r), at] = (gate / (1.0 + jnp.exp(-gate)) * up).astype(BF16)
-            return 0
-
-        lax.fori_loop(0, hidden // wide, unit, 0)
+
+        wide_steps(act)
 
     blocks = 2 * feeder.dims[0] * feeder.dims[1]
     held = blocks // 2
@@ -578,7 +577,7 @@
         return jnp.logical_and(holds, there)
 
     def lent(s, b, r):
-        at = (s * blocks + b) * chunks + r
+        at = (s * held + lax.rem(b, held)) * chunks + r
         local = of(lax.rem(b, held), span)
         return to(
             peer,
@@ -589,7 +588,7 @@
         )
 
     def sends(b, r):
-        at = b * chunks + r
+        at = lax.rem(b, held) * chunks + r
         local = of(lax.rem(b, held), span)
         return to(
             across,
@@ -634,15 +633,11 @@
 
     @scoped
     def down(late, r):
-        ahead = None
         for j, spot in units[late]:
             landed(j, spot)
             guarded(inside(spot), functools.partial(term, 1, j, spot, r))
-            if ahead:
-                settle(*ahead, r)
-            ahead = (j, spot)
-        if ahead:
-            settle(*ahead, r)
+        for j, spot in units[late]:
+            settle(j, spot, r)
 
     @scoped
     def down_own(late):
@@ -675,21 +670,22 @@
         for copy in seq_beside:
             copy.start()
 
-    @scoped
     def m_cross_start():
+        m_ready()
         for copy in m_cross:
             copy.start()
 
     @scoped
     def m_wait():
-        for copy in own[:2]:
-            copy.wait()
         for copy in m_landed:
             copy.wait_recv()
 
+    def d_cross_start():
+        d_ready()
+        d_cross.start()
+
     @scoped
     def d_wait():
-        own[2].wait()
         d_landed.wait_recv()
 
     @scoped
@@ -706,53 +702,55 @@
         if s == 0:
             seq_local.wait()
             seq_peer.wait_recv()
-        norm(both.at[s], s, 0, length, 0)
-
-    def finished(part):
-        finish(part)
-        if part in inputs:
-            own[3 + sorted(inputs).index(part)].wait()
-
-    def relays(part, depth):
-        if depth < deepest[part]:
-            relay(part, depth)
+        norm(both.at[s], s, 0, length, mix_gain)
 
     acts = {
-        "launch": launch,
-        "relay": relays,
-        "finish": finished,
-        "seq": seq_start,
-        "m_cross": m_cross_start,
-        "m_wait": m_wait,
-        "d_cross": lambda: d_cross.start(),
-        "d_wait": d_wait,
-        "pass_seq": pass_seq,
-        "seq_wait": seq_wait,
-        "norm": norm_of,
-        "project": project,
-        "scales": scales,
-        "mix_terms": mix_terms,
-        "mix_cross": mix_cross,
-        "mix_after": mix_after,
-        "pass_on": pass_on,
-        "feed": feed,
-        "E": functools.partial(down, 0),
-        "L": functools.partial(down, 1),
-        "Z": down_own,
-        "end": end,
+        LAUNCH: launch,
+        RELAY: relay,
+        FINISH: finish,
+        ROWS_SWAP: seq_start,
+        MIX_SWAP: m_cross_start,
+        MIX_WAIT: m_wait,
+        DOWN_SWAP: d_cross_start,
+        DOWN_WAIT: d_wait,
+        ROWS_PASS: pass_seq,
+        ROWS_WAIT: seq_wait,
+        NORM: norm_of,
+        PROJECT: project,
+        SCALES: scales,
+        MIX_AWAY: functools.partial(mix_terms, 1),
+        MIX_OWN: functools.partial(mix_terms, 0),
+        MIX_SEND: mix_cross,
+        MIX_AFTER: mix_after,
+        AFTER_PASS: pass_on,
+        FEED_UP: feed_up,
+        FEED_GATE: feed,
+        DOWN_NEAR: functools.partial(down, 0),
+        DOWN_FAR: functools.partial(down, 1),
+        DOWN_OWN: down_own,
+        END: end,
     }
     seq_peer.start()
     seq_local.start()
-    for copy in own:
-        copy.start()
-    extra = max(deepest) - 1
-    for line in ORDER.split(";"):
-        name, *given = line.split()
-        given = [int(g) for g in given]
+    p_ready()
+    g_done = False
+    for number, (name, *given) in enumerate(ORDER):
+        if name == LAUNCH:
+            if given[0] in (4, 5) and not g_done:
+                g_done = True
+                g_ready()
+            if full[0] < 4:
+                if any(o[:2] == (LAUNCH, given[0]) for o in ORDER[:number]):
+                    continue
+                given = given[:1]
+        if name == RELAY and given[1] >= len(forks[given[0]]):
+            continue
         acts[name](*given)
-        if name == "relay" and given[1] == 3:
-            for depth in range(4, extra + 1):
-                relays(given[0], depth)
+        if name == RELAY and all(o[:2] != (RELAY, given[0]) for o in ORDER[number + 1 :]):
+            known = {o[2] for o in ORDER if o[:2] == (RELAY, given[0])}
+            for fork in range(len(forks[given[0]])):
+                if fork not in known:
+                    relay(given[0], fork)
     for part, number, holds in sent:
         guarded(holds, copy_of(part, number).wait_send)
     seq_peer.wait_send()
@@ -775,8 +773,35 @@
     each(drain)
 
 
-def prepare(
-    full,
+def prepare(full, xp, yp, proj_scales, taps, mix_out_scale, down_scale, ffn_scales, kch, units):
+    half = full[0] * full[1] * full[2] // 2
+    lines, columns = half // full[2], full[2]
+    cols = mix_out_scale.shape[0]
+    wide = half * kch
+    thin = []
+    for scale in (mix_out_scale, down_scale):
+        high = lax.reduce_precision(scale, 8, 7)
+        middle = lax.reduce_precision(scale - high, 8, 7)
+        thin += [high, middle, scale - high - middle]
+    thin = jnp.stack(thin)
+    ours = (lax.iota(jnp.int32, 2 * cols) // cols == xp)[None]
+    thin = jnp.where(ours, jnp.concatenate([thin, thin], 1), 0.0).astype(BF16)
+    thin = jnp.pad(thin, ((0, 10), (0, 2 * wide - 2 * cols)))
+    chan = jnp.concatenate([proj_scales, taps]).reshape(6, half, 2, 2, kch)
+    chan = lax.dynamic_index_in_dim(chan, xp, 2, keepdims=False)
+    chan = chan.transpose(2, 0, 1, 3).reshape(2, 6, wide)
+    chan = jnp.pad(chan, ((0, 0), (0, 2), (0, 0)))
+    hid = ffn_scales.reshape(2, lines, 2, columns, units)
+    hid = lax.dynamic_index_in_dim(hid, yp, 2, keepdims=False)
+    hid = jnp.pad(hid, ((0, 6), (0, 0), (0, 0), (0, -units % 16))).reshape(8, -1)
+    return thin, chan, hid
+
+
+def body(
+    n,
+    sequence,
+    mix_gain,
+    ffn_gain,
     proj_outer,
     proj_inner,
     proj_value,
@@ -790,64 +815,43 @@
     ffn_down,
     down_scale,
 ):
-    half = full[0] * full[1] * full[2] // 2
-    lines, columns = half // full[2], full[2]
-    me = lax.axis_index("fs")
-    xp, yp = lax.rem(me, 2), lax.rem(me // columns, 2)
-    each = proj_outer.shape[1]
-    kch = each // 2
-    p_in = jnp.stack(
-        [w.astype(BF16).T.reshape(2, kch, -1) for w in (proj_outer, proj_inner, proj_value)],
-        axis=1,
-    )
-    units = ffn_gate.shape[1]
-    fill = -units % 16
-    g_in = jnp.stack(
-        [jnp.pad(w.astype(BF16).T, ((0, fill), (0, 0))) for w in (ffn_gate, ffn_up)]
-    )
-    cols = mix_out.shape[1]
-    mixed = mix_out.astype(BF16).T.reshape(cols, half, 2, 2, kch)
-    mixed = mixed.transpose(2, 0, 3, 1, 4).reshape(2, cols, half * each)
-    thin = []
-    for scale in (mix_out_scale, down_scale):
-        high = lax.reduce_precision(scale, 8, 7)
-        middle = lax.reduce_precision(scale - high, 8, 7)
-        thin += [high, middle, scale - high - middle]
-    thin = jnp.stack(thin)
-    ours = (lax.iota(jnp.int32, 2 * cols) // cols == xp)[None]
-    thin = jnp.where(ours, jnp.concatenate([thin, thin], 1), 0.0).astype(BF16)
-    thin = jnp.pad(thin, ((0, 10), (0, half * each - 2 * cols)))
-    m_in = jnp.concatenate([mixed, jnp.broadcast_to(thin, (2,) + thin.shape)], axis=1)
-    down = ffn_down.astype(BF16).T.reshape(cols, lines, 2, columns, units)
-    down = jnp.pad(down, ((0, 0), (0, 0), (0, 0), (0, 0), (0, fill)))
-    d_in = down.transpose(2, 0, 1, 3, 4).reshape(2, cols, -1)
-    chan = jnp.concatenate([proj_scales, taps]).reshape(6, half, 2, 2, kch)
-    chan = lax.dynamic_index_in_dim(chan, xp, 2, keepdims=False)
-    chan = chan.transpose(2, 0, 1, 3).reshape(2, 6, half * kch)
-    chan = jnp.pad(chan, ((0, 0), (0, 2), (0, 0)))
-    hid = ffn_scales.reshape(2, lines, 2, columns, units)
-    hid = lax.dynamic_index_in_dim(hid, yp, 2, keepdims=False)
-    hid = jnp.pad(hid, ((0, 6), (0, 0), (0, 0), (0, fill))).reshape(8, -1)
-    return p_in, m_in, g_in, d_in, chan, hid
-
-
-def body(n, sequence, mix_gain, ffn_gain, *rest):
     seq = sequence[0]
     length, width = seq.shape
     depth = 2 * width
     full = grid_of(n)
-    p_in, m_in, g_in, d_in, chan, hid = prepare(full, *rest)
-    gains = jnp.pad(jnp.stack([mix_gain, ffn_gain]), ((0, 6), (0, 0)))
+    me = lax.axis_index("fs")
+    xp, yp = lax.rem(me, 2), lax.rem(me // full[2], 2)
+    kch, units_in = proj_outer.shape[1] // 2, ffn_gate.shape[1]
+    thin, chan, hid = prepare(
+        full, xp, yp, proj_scales, taps, mix_out_scale, down_scale, ffn_scales, kch, units_in
+    )
     members = n // 2
-    kch, fch = p_in.shape[2], g_in.shape[1]
-    cols = m_in.shape[1] - 16
+    fch = units_in + -units_in % 16
+    cols = mix_out.shape[1]
+    ours = 2 * kch * members
     chunks = length // ROWS
     units = members * fch
-    items = len(ORDERS) * 4 * members
-    operands = (seq, p_in, m_in, g_in, d_in, chan, gains, hid)
-    sems = [pltpu.SemaphoreType.DMA((k,)) for k in (items,)]
-    sems += [pltpu.SemaphoreType.DMA((len(ORDERS), members)), pltpu.SemaphoreType.DMA((8,))]
-    for k in (4 + 2 * chunks, 2 * chunks, 4 * chunks, 2 * n * chunks, n * chunks):
+    dims = [tuple(d // 2 if k == h else d for k, d in enumerate(full)) for h in (X, Y)]
+    items = sum(len(routes(dims[g], order)) for g, order in ORDERS)
+    held = full[0] * (full[1] // 2)
+    operands = (
+        seq,
+        proj_outer.T,
+        proj_inner.T,
+        proj_value.T,
+        mix_out,
+        ffn_gate.T,
+        ffn_up.T,
+        ffn_down,
+        thin,
+        chan,
+        mix_gain[None],
+        ffn_gain[None],
+        hid,
+    )
+    sems = [pltpu.SemaphoreType.DMA((items,))]
+    sems += [pltpu.SemaphoreType.DMA((len(ORDERS), members)), pltpu.SemaphoreType.DMA((1,))]
+    for k in (4 + 2 * chunks, 2 * chunks, 4 * chunks, 2 * held * chunks, held * chunks):
         sems += [pltpu.SemaphoreType.DMA((k,))] * 2
     result = pl.pallas_call(
         functools.partial(layer_kernel, full),
@@ -856,16 +860,20 @@
         out_specs=pl.BlockSpec(memory_space=pltpu.VMEM),
         scratch_shapes=[
             pltpu.VMEM((2, 3, members * kch, depth), BF16),
-            pltpu.VMEM((members, 2 * cols + 32, m_in.shape[2]), BF16),
+            pltpu.VMEM((members, 2 * cols + 32, ours), BF16),
             pltpu.VMEM((2, units, depth), BF16),
             pltpu.VMEM((2, members * cols, units), BF16),
             pltpu.VMEM((2, length, depth), BF16),
             pltpu.VMEM((length, depth), BF16),
             pltpu.VMEM((2, length, depth), BF16),
-            pltpu.VMEM((2, length, m_in.shape[2]), BF16),
+            pltpu.VMEM((2, length, ours), BF16),
             pltpu.VMEM((8 + ROWS, members * kch), F32),
             pltpu.VMEM((2, length, units), BF16),
             pltpu.VMEM((8, depth), F32),
+            pltpu.VMEM((cols, ours), BF16),
+            pltpu.VMEM((cols, units), BF16),
+            pltpu.VMEM((ours, cols), F32),
+            pltpu.VMEM((units, cols), F32),
             pltpu.VMEM((2, length, width), BF16),
             pltpu.VMEM((2, length, width), BF16),
             pltpu.VMEM((2, length, width), BF16),

time: 240 us -> 219 us (0.912)
  Pallas kernels: 226 us -> 211 us
  other arithmetic: 6.84 us -> 1.44 us
    pallas_call x1, Pallas kernels: 226 us -> 211 us  [body(): pl.pallas_call(functools.partial(layer_kernel, full), out_shape=jax.Shape...]
    another operation x3 -> x0, other arithmetic: 3.28 us -> none  [the longest x1 1.35 us: body(): gains = jnp.pad(jnp.stack([mix_gain, ffn_gain]), ((0, 6), (0, 0)))]
where the time goes in v2:
time: 219 us
  Pallas kernels  211 us (96%)
  local copies, waits for them, and re-layouts  5.69 us (3%)
    pallas_call x1, Pallas kernels, body(): pl.pallas_call(functools.partial(layer_kernel, full), out_shape=jax.Shape...  211 us

profile of v2, /device:TPU:1, one launch (start us, length us, event | category | flops | bytes accessed | tf_op | source)
XLA Modules:
  0.0 218.5 jit_solution(13337467083496156392)
XLA Ops:
  0.0 0.7 fusion.2
  0.7 0.6 pad.12.thin
  1.3 0.8 reshape.28
  2.2 0.7 reshape.29.hid
  2.9 0.7 pad_maximum_fusion
  3.6 0.1 reshape.26
  3.8 0.1 reshape.27
  3.9 0.6 pad.13.chan
  4.5 211.3 %layer.1 = bf16[768,1024]{1,0:T(8,128)(2,1)} custom-call(bf16[768,1024]{1,0:T(8,128)(2,1)} %bitcast.33, f32[64,2048]{1,0:T(8,128)} %bitcast.36, f32[64,2048]{1,0:T(8,128)} %bitcast.37, f32[64,2048]{1,0:T(8,128)} %bitcast.38, f32[1024,128]{1,0:T(8,128)} %m_in.1, f32[88,2048]{1,0:T(8,128)} %bitcast.34, f32[88,2048]{1,0:T(8,128)} %bitcast.35, ...), custom_call_target="tpu_custom_call" | custom-call | tf_op jit(solution)/shard_map/layer/pallas_call | solution.py:856
  215.8 2.7 %copy.22 = bf16[1,768,1024]{2,1,0:T(8,128)(2,1)} copy(bf16[1,768,1024]{2,1,0:T(8,128)(2,1)} %bitcast.32) | data formatting | bytes 3145728
  (8 shorter events, 0.1 us)

commit v3 on v2

--- a/solution.py
+++ b/solution.py
@@ -149,27 +149,27 @@
 ) = range(24)
 
 ORDER = (
-    (LAUNCH, 1, 0), (LAUNCH, 1, 1), (MIX_SWAP,), (DOWN_SWAP,), (LAUNCH, 5, 2), (NORM, 0), (MIX_WAIT,),
-    (LAUNCH, 3, 0), (RELAY, 1, 0), (RELAY, 1, 1), (LAUNCH, 0, 0), (LAUNCH, 4, 2), (RELAY, 1, 3),
-    (LAUNCH, 3, 1), (DOWN_WAIT,), (RELAY, 1, 2), (RELAY, 3, 1), (ROWS_SWAP,), (RELAY, 3, 0),
-    (RELAY, 1, 4), (RELAY, 3, 2), (RELAY, 3, 4), (LAUNCH, 2, 0), (RELAY, 2, 0), (LAUNCH, 6, 2), (RELAY, 1, 5),
-    (RELAY, 3, 3), (RELAY, 3, 5), (LAUNCH, 5, 0), (RELAY, 0, 1), (LAUNCH, 7, 2), (FINISH, 1),
-    (PROJECT, 1, 0), (RELAY, 0, 0), (RELAY, 2, 1), (FINISH, 3), (RELAY, 5, 1), (ROWS_PASS, 0),
-    (ROWS_PASS, 1), (RELAY, 5, 0), (LAUNCH, 0, 1), (RELAY, 2, 3), (RELAY, 0, 3), (RELAY, 0, 2),
-    (LAUNCH, 4, 0), (RELAY, 0, 4), (ROWS_PASS, 2), (RELAY, 2, 5), (ROWS_WAIT,), (RELAY, 2, 2),
-    (RELAY, 5, 2), (NORM, 1), (RELAY, 5, 3), (RELAY, 0, 5), (RELAY, 4, 1), (LAUNCH, 2, 1), (PROJECT, 1, 1),
-    (RELAY, 5, 5), (RELAY, 2, 4), (RELAY, 4, 0), (FINISH, 0), (PROJECT, 0, 1), (RELAY, 5, 4), (FINISH, 2),
-    (SCALES,), (RELAY, 6, 0), (LAUNCH, 6, 0), (MIX_AWAY, 0), (MIX_AWAY, 1), (MIX_AWAY, 2),
-    (MIX_SEND, 0), (MIX_SEND, 1), (LAUNCH, 7, 0), (MIX_SEND, 2), (PROJECT, 0, 0), (MIX_OWN, 0),
-    (RELAY, 4, 3), (MIX_OWN, 2), (RELAY, 6, 3), (MIX_OWN, 1), (MIX_AFTER, 0), (RELAY, 6, 4),
-    (MIX_AFTER, 1), (RELAY, 7, 0), (RELAY, 7, 1), (FINISH, 5), (FEED_UP, 0, 1), (FEED_UP, 0, 0),
-    (RELAY, 4, 2), (RELAY, 4, 4), (RELAY, 4, 5), (MIX_AFTER, 2), (RELAY, 7, 3), (RELAY, 6, 1), (RELAY, 7, 4),
-    (FEED_UP, 0, 2), (AFTER_PASS, 0), (AFTER_PASS, 1), (RELAY, 7, 2), (FEED_UP, 1, 0), (RELAY, 6, 2),
-    (FEED_UP, 1, 1), (RELAY, 7, 7), (FINISH, 4), (FEED_GATE, 1, 0), (RELAY, 6, 8), (AFTER_PASS, 2),
-    (RELAY, 7, 5), (RELAY, 7, 6), (DOWN_NEAR, 0), (RELAY, 6, 5), (FEED_GATE, 1, 1), (DOWN_NEAR, 1),
-    (RELAY, 7, 8), (FEED_UP, 1, 2), (FEED_GATE, 1, 2), (RELAY, 6, 7), (RELAY, 6, 6), (DOWN_FAR, 0),
-    (DOWN_FAR, 1), (FEED_GATE, 0, 0), (FEED_GATE, 0, 1), (DOWN_NEAR, 2), (DOWN_FAR, 2),
-    (FEED_GATE, 0, 2), (DOWN_OWN, 0), (DOWN_OWN, 1), (END,),
+    (LAUNCH, 1, 0), (LAUNCH, 1, 1), (MIX_SWAP,), (MIX_WAIT,), (ROWS_SWAP,), (DOWN_SWAP,),
+    (LAUNCH, 5, 2), (LAUNCH, 3, 0), (RELAY, 1, 0), (RELAY, 1, 1), (RELAY, 3, 0), (RELAY, 3, 1),
+    (DOWN_WAIT,), (LAUNCH, 7, 2), (LAUNCH, 6, 2), (LAUNCH, 2, 0), (LAUNCH, 3, 1), (RELAY, 3, 2),
+    (RELAY, 1, 2), (RELAY, 3, 4), (RELAY, 3, 3), (RELAY, 1, 3), (RELAY, 3, 5), (LAUNCH, 0, 0), (LAUNCH, 4, 2),
+    (LAUNCH, 5, 0), (LAUNCH, 0, 1), (RELAY, 1, 5), (ROWS_PASS, 0), (RELAY, 0, 1), (LAUNCH, 2, 1),
+    (ROWS_PASS, 1), (RELAY, 0, 0), (RELAY, 1, 4), (FINISH, 3), (RELAY, 0, 2), (ROWS_PASS, 2),
+    (RELAY, 0, 4), (FINISH, 1), (RELAY, 2, 0), (ROWS_WAIT,), (NORM, 1), (PROJECT, 1, 1), (RELAY, 2, 2),
+    (RELAY, 5, 0), (RELAY, 2, 1), (RELAY, 0, 3), (RELAY, 5, 1), (NORM, 0), (RELAY, 0, 5), (RELAY, 2, 4),
+    (RELAY, 2, 3), (LAUNCH, 4, 0), (RELAY, 5, 2), (RELAY, 2, 5), (RELAY, 6, 0), (RELAY, 5, 3), (RELAY, 4, 0),
+    (LAUNCH, 6, 0), (RELAY, 4, 1), (FINISH, 0), (PROJECT, 0, 1), (FINISH, 2), (SCALES,), (MIX_AWAY, 0),
+    (MIX_AWAY, 1), (LAUNCH, 7, 0), (MIX_AWAY, 2), (MIX_SEND, 0), (MIX_SEND, 1), (MIX_SEND, 2),
+    (RELAY, 5, 5), (RELAY, 6, 4), (PROJECT, 1, 0), (RELAY, 7, 0), (PROJECT, 0, 0), (RELAY, 5, 4),
+    (MIX_OWN, 0), (MIX_AFTER, 0), (RELAY, 4, 3), (MIX_OWN, 1), (MIX_AFTER, 1), (RELAY, 4, 2),
+    (RELAY, 7, 3), (RELAY, 6, 2), (AFTER_PASS, 0), (RELAY, 4, 4), (FINISH, 5), (RELAY, 7, 2), (RELAY, 6, 8),
+    (FEED_UP, 1, 0), (MIX_OWN, 2), (RELAY, 6, 6), (FEED_UP, 0, 1), (MIX_AFTER, 2), (AFTER_PASS, 1),
+    (RELAY, 4, 5), (RELAY, 6, 3), (RELAY, 7, 7), (FEED_UP, 1, 1), (RELAY, 7, 4), (RELAY, 7, 1), (RELAY, 6, 7),
+    (RELAY, 6, 1), (FINISH, 4), (FEED_GATE, 1, 0), (DOWN_NEAR, 0), (AFTER_PASS, 2), (FEED_GATE, 1, 1),
+    (DOWN_NEAR, 1), (FEED_UP, 1, 2), (FEED_GATE, 1, 2), (DOWN_NEAR, 2), (RELAY, 7, 8), (RELAY, 7, 6),
+    (RELAY, 7, 5), (RELAY, 6, 5), (DOWN_FAR, 0), (DOWN_FAR, 1), (FEED_UP, 0, 2), (FEED_UP, 0, 0),
+    (DOWN_FAR, 2), (FEED_GATE, 0, 0), (FEED_GATE, 0, 1), (FEED_GATE, 0, 2), (DOWN_OWN, 0), (DOWN_OWN, 1),
+    (END,),
 )
 
 
@@ -790,10 +790,9 @@
     chan = jnp.concatenate([proj_scales, taps]).reshape(6, half, 2, 2, kch)
     chan = lax.dynamic_index_in_dim(chan, xp, 2, keepdims=False)
     chan = chan.transpose(2, 0, 1, 3).reshape(2, 6, wide)
-    chan = jnp.pad(chan, ((0, 0), (0, 2), (0, 0)))
     hid = ffn_scales.reshape(2, lines, 2, columns, units)
     hid = lax.dynamic_index_in_dim(hid, yp, 2, keepdims=False)
-    hid = jnp.pad(hid, ((0, 6), (0, 0), (0, 0), (0, -units % 16))).reshape(8, -1)
+    hid = jnp.pad(hid, ((0, 0), (0, 0), (0, 0), (0, -units % 16))).reshape(2, -1)
     return thin, chan, hid
 
 

time: 219 us -> 219 us (level)
  no operation moved by 1% of the time
where the time goes in v3:
time: 219 us
  Pallas kernels  211 us (96%)
  local copies, waits for them, and re-layouts  5.65 us (3%)
    pallas_call x1, Pallas kernels, body(): pl.pallas_call(functools.partial(layer_kernel, full), out_shape=jax.Shape...  211 us

profile of v3, /device:TPU:1, one launch (start us, length us, event | category | flops | bytes accessed | tf_op | source)
XLA Modules:
  0.0 218.6 jit_solution(15959823519626931263)
XLA Ops:
  0.0 0.7 fusion.2
  0.7 0.6 pad.8.thin
  1.3 0.8 reshape.28
  2.2 0.7 reshape.29.hid
  2.9 0.7 pad_maximum_fusion
  3.6 0.1 reshape.26
  3.8 0.1 reshape.27
  3.9 0.6 copy.18.chan
  4.5 211.5 %layer.1 = bf16[768,1024]{1,0:T(8,128)(2,1)} custom-call(bf16[768,1024]{1,0:T(8,128)(2,1)} %bitcast.33, f32[64,2048]{1,0:T(8,128)} %bitcast.36, f32[64,2048]{1,0:T(8,128)} %bitcast.37, f32[64,2048]{1,0:T(8,128)} %bitcast.38, f32[1024,128]{1,0:T(8,128)} %m_in.1, f32[88,2048]{1,0:T(8,128)} %bitcast.34, f32[88,2048]{1,0:T(8,128)} %bitcast.35, ...), custom_call_target="tpu_custom_call" | custom-call | tf_op jit(solution)/shard_map/layer/pallas_call | solution.py:855
  216.0 2.7 %copy.22 = bf16[1,768,1024]{2,1,0:T(8,128)(2,1)} copy(bf16[1,768,1024]{2,1,0:T(8,128)(2,1)} %bitcast.32) | data formatting | bytes 3145728
  (7 shorter events, 0.1 us)
